TPU v7x, 32 devices: a whole 2x2x4 slice. The times are simulated.
32 devices in a mesh: sp: 8 (over z, y), tp: 4 (over x, core).
Axes of the slice: x: 2, y: 2, z: 4, core: 2. Of those that a mesh axis runs over, the one named last changes fastest.
Arguments:
- residual: bfloat16 [2048, 2048], P('sp'), may hold values from -6 to 6
- ssm_input: bfloat16 [2048, 1024], P('sp', 'tp'), may hold values from -6 to 6
- in_map: bfloat16 [2, 64, 16, 128], P(None, 'tp'), may hold values from -1 to 1
- out_map: bfloat16 [2, 64, 16, 128], P(None, 'tp'), may hold values from -0.5 to 0.5
- damping: float32 [64, 64], P('tp'), may hold values from 0.0001 to 0.24
- log_step: float32 [64], P('tp'), may hold values from -8 to -1.2
- frequency: float32 [64, 64], P('tp'), may hold values from 1 to 201.06177
- pacing: float32 [2048], P('sp'), may hold values from 0.28 to 3.5
- feedthrough: float32 [1024], P('tp'), may hold values from -4 to 4
- w_out: bfloat16 [1024, 2048], P('tp'), may hold values from -0.375 to 0.375
- gain_mix: float32 [2048], replicated, may hold values from 0.1 to 1.9
- w_gate: bfloat16 [2048, 5632], P('sp', 'tp'), may hold values from -0.125 to 0.125
- w_value: bfloat16 [2048, 5632], P('sp', 'tp'), may hold values from -0.125 to 0.125
- conv_taps: float32 [3, 5632], P(None, 'tp'), may hold values from -3 to 3
- w_down: bfloat16 [5632, 2048], P('tp', 'sp'), may hold values from -0.21875 to 0.21875
- gain_ffn: float32 [2048], replicated, may hold values from 0.1 to 1.9
Outputs:
- result: bfloat16 [2048, 2048], P(('sp', 'tp'))
All inputs are finite; a program needn't handle non-finite values.
Results may differ from a plain program's by a relative error of at most 0.02.
Values may be sent and summed in bfloat16 or wider, within the bound.
A program may use at most 128 MiB of HBM per device.

v0:
```python
import math

import jax
import jax.numpy as jnp
from jax import lax
from jax.sharding import PartitionSpec as P

deep_alpha = 8.0**0.25
norm_eps = 1e-06
highest = lax.Precision.HIGHEST


def carried_in(value, axis, join, neutral, backward):
    count, mine = (lax.axis_size(axis), lax.axis_index(axis))
    pieces = jax.tree.map(lambda part: lax.all_gather(part, axis), value)
    if backward:
        pieces = jax.tree.map(lambda part: part[::-1], pieces)
        mine = count - 1 - mine
    total = jax.tree.map(
        lambda part, zero: jnp.full_like(part, 0) + jnp.asarray(zero, part.dtype), value, neutral
    )

    def hop(position, total):
        longer = join(total, jax.tree.map(lambda part: part[position], pieces))
        return jax.tree.map(lambda new, old: jnp.where(position < mine, new, old), longer, total)

    return lax.fori_loop(0, count - 1, hop, total)


def extended(cells, sides, width):
    for axis, dim in sides:
        count = lax.axis_size(axis)
        ends = count - 1
        head = lax.slice_in_dim(cells, 0, width, axis=dim)
        tail = lax.slice_in_dim(cells, cells.shape[dim] - width, cells.shape[dim], axis=dim)
        cells = jnp.concatenate(
            [
                lax.ppermute(tail, axis, [(i, (i + 1) % count) for i in range(ends)]),
                cells,
                lax.ppermute(head, axis, [((i + 1) % count, i) for i in range(ends)]),
            ],
            axis=dim,
        )
    return cells


def normalize(pre_norm, gain_row):
    mean_row = jnp.mean(pre_norm, axis=-1, keepdims=True)
    centred = pre_norm - mean_row
    spread = jnp.mean(centred * centred, axis=-1, keepdims=True)
    return centred * lax.rsqrt(spread + norm_eps) * gain_row


def complex_mul(first_pair, second_pair):
    state_half = first_pair.shape[-1] // 2
    a_re = first_pair[..., :state_half]
    a_im = first_pair[..., state_half:]
    b_re = second_pair[..., :state_half]
    b_im = second_pair[..., state_half:]
    return jnp.concatenate([a_re * b_re - a_im * b_im, a_re * b_im + a_im * b_re], axis=-1)


def combine_pair(earlier, later):
    return (complex_mul(earlier[0], later[0]), complex_mul(later[0], earlier[1]) + later[1])


def unit_pair(groups, state_half):
    return jnp.concatenate(
        [jnp.ones((groups, state_half), jnp.float32), jnp.zeros((groups, state_half), jnp.float32)],
        axis=-1,
    )


def local_pass(u_rows, pace_rows, in_map_d, pair_re, pair_im, rate_inv, phase_shift):
    positions = u_rows.shape[0]
    groups = u_rows.shape[1]
    state_pair = pair_re.shape[1]
    block_len = min(64, positions)
    blocks = positions // block_len
    identity_pair = unit_pair(groups, state_pair // 2)
    inflow = jnp.einsum("tgc,gcq->tgq", u_rows, in_map_d, preferred_element_type=jnp.float32)
    deltas = pace_rows[:, None, None]
    decays = jnp.exp(pair_re * deltas) * jnp.cos(pair_im * deltas - phase_shift)
    driven = complex_mul(complex_mul(decays - identity_pair, rate_inv), inflow)
    within = jnp.cumsum(pace_rows.reshape(blocks, block_len), axis=1)[:, :, None, None]
    advance = jnp.exp(pair_re * within) * jnp.cos(pair_im * within - phase_shift)
    inverse = jnp.exp(-pair_re * within) * jnp.cos(pair_im * within + phase_shift)
    weighted = complex_mul(inverse, driven.reshape(blocks, block_len, groups, state_pair))
    triangle = (
        lax.broadcasted_iota(jnp.int32, (block_len, block_len), 0)
        >= lax.broadcasted_iota(jnp.int32, (block_len, block_len), 1)
    ).astype(jnp.float32)
    running = jnp.einsum(
        "st,btq->bsq",
        triangle,
        weighted.reshape(blocks, block_len, groups * state_pair),
        precision=highest,
    )
    running = running.reshape(blocks, block_len, groups, state_pair)

    def carry_step(state_now, block_terms):
        level_now, product_now = state_now
        total_now, end_now = block_terms
        return (
            (complex_mul(end_now, level_now + total_now), complex_mul(end_now, product_now)),
            (level_now, product_now),
        )

    start_pair = (jnp.zeros_like(identity_pair), identity_pair)
    last_pair, outputs = lax.scan(carry_step, start_pair, (running[:, -1], advance[:, -1]))
    return (advance, running, outputs[0], outputs[1], last_pair[1], last_pair[0])


def finish(pass_out, incoming, out_map_d):
    advance = pass_out[0]
    running = pass_out[1]
    starts = pass_out[2] + complex_mul(pass_out[3], incoming[None])
    states = complex_mul(advance, starts[:, None] + running)
    readout = jnp.einsum("bsgq,gcq->bsgc", states, out_map_d.astype(jnp.float32), precision=highest)
    return readout.reshape(readout.shape[0] * readout.shape[1], readout.shape[2], readout.shape[3])


def shards(
    residual,
    ssm_input,
    in_map,
    out_map,
    damping,
    log_step,
    frequency,
    pacing,
    feedthrough,
    w_out,
    gain_mix,
    w_gate,
    w_value,
    conv_taps,
    w_down,
    gain_ffn,
):
    positions = ssm_input.shape[0]
    channel_count = ssm_input.shape[1]
    groups = damping.shape[0]
    state_half = damping.shape[1]
    group_width = channel_count // groups
    own_rows = positions // lax.axis_size("tp")
    phase_shift = jnp.concatenate(
        [jnp.zeros((state_half,), jnp.float32), jnp.full((state_half,), 0.5 * math.pi, jnp.float32)]
    )
    rate_re = -damping
    step_col = jnp.exp(log_step)[:, None]
    pair_re = jnp.concatenate([rate_re, rate_re], axis=-1) * step_col
    pair_im = jnp.concatenate([frequency, frequency], axis=-1) * step_col
    modulus = rate_re * rate_re + frequency * frequency
    rate_inv = jnp.concatenate([rate_re / modulus, -frequency / modulus], axis=-1)
    u_rows = ssm_input.reshape(positions, groups, group_width)
    forward_pass = local_pass(u_rows, pacing, in_map[0], pair_re, pair_im, rate_inv, phase_shift)
    backward_pass = local_pass(
        u_rows[::-1], pacing[::-1], in_map[1], pair_re, pair_im, rate_inv, phase_shift
    )
    identity = (unit_pair(groups, state_half), jnp.zeros((groups, 2 * state_half), jnp.float32))
    forward_in = carried_in((forward_pass[4], forward_pass[5]), "sp", combine_pair, identity, False)
    backward_in = carried_in(
        (backward_pass[4], backward_pass[5]), "sp", combine_pair, identity, True
    )
    readout = (
        finish(forward_pass, forward_in[1], out_map[0])
        + finish(backward_pass, backward_in[1], out_map[1])[::-1]
    )
    readout = readout.reshape(positions, channel_count) + feedthrough * ssm_input.astype(
        jnp.float32
    )
    channels = jax.nn.gelu(readout).astype(jnp.bfloat16)
    mixed = lax.psum(
        jnp.dot(channels, w_out, preferred_element_type=jnp.float32).astype(jnp.bfloat16), "tp"
    ).astype(jnp.float32)
    whole_rows = normalize(deep_alpha * residual.astype(jnp.float32) + mixed, gain_mix).astype(
        jnp.bfloat16
    )
    norm_first = lax.dynamic_slice_in_dim(whole_rows, lax.axis_index("tp") * own_rows, own_rows, 0)
    first_kept = lax.optimization_barrier(norm_first).astype(jnp.float32)
    gate_sum = jnp.dot(
        whole_rows,
        lax.all_gather(w_gate, "sp", axis=0, tiled=True),
        preferred_element_type=jnp.float32,
    )
    value_sum = jnp.dot(
        whole_rows,
        lax.all_gather(w_value, "sp", axis=0, tiled=True),
        preferred_element_type=jnp.float32,
    )
    gated = gate_sum.astype(jnp.bfloat16)
    values = lax.optimization_barrier(value_sum.astype(jnp.bfloat16)).astype(jnp.float32)
    padded = extended(gated, (("sp", 0),), 1).astype(jnp.float32)
    smoothed = conv_taps[0] * padded[:-2] + conv_taps[1] * padded[1:-1] + conv_taps[2] * padded[2:]
    hidden = (jax.nn.gelu(smoothed) * values).astype(jnp.bfloat16)
    partials = jnp.dot(
        hidden, lax.all_gather(w_down, "sp", axis=1, tiled=True), preferred_element_type=jnp.float32
    )
    branch = lax.psum_scatter(
        partials.astype(jnp.bfloat16), "tp", scatter_dimension=0, tiled=True
    ).astype(jnp.float32)
    return normalize(deep_alpha * first_kept + branch, gain_ffn).astype(jnp.bfloat16)


def solution(mesh):
    in_specs = (
        P("sp", None),
        P("sp", "tp"),
        P(None, "tp", None, None),
        P(None, "tp", None, None),
        P("tp", None),
        P("tp"),
        P("tp", None),
        P("sp"),
        P("tp"),
        P("tp", None),
        P(),
        P("sp", "tp"),
        P("sp", "tp"),
        P(None, "tp"),
        P("tp", "sp"),
        P(),
    )
    out_specs = P(("sp", "tp"), None)
    return jax.shard_map(shards, mesh=mesh, in_specs=in_specs, out_specs=out_specs, check_vma=False)
```

profile of v0, /device:TPU:0, one launch (start us, length us, event | category | flops | bytes accessed | tf_op | source)
XLA Modules:
  0.0 552.3 jit_solution(3094445604148882098)
XLA Ops:
  13.1 1.8 convolution_bitcast_fusion
  15.2 14.3 %multiply_add_fusion.12 = (f32[256,16,128]{0,2,1:T(8,128)S(1)}, f32[256,16,128]{0,2,1:T(8,128)S(1)}) fusion(f32[256]{0:T(256)S(1)} %rev.15, f32[16,128]{1,0:T(8,128)S(1)} %copy-done.23, f32[128]{0:T(128)S(1)} %copy-done.25, f32[16,128]{1,0:T(8,128)S(1)} %get-tuple-element.459, f32[16,128]{1,0:T(8,128)S(1)} %get-tuple-element.399, f32[256]{0:T(256)S(1)} %copy-done.20), kind=kLoop, calls=%fused_computation.76 | loop fusion | flops 5242880 | bytes 4221440 | tf_op jit(solution)/shard_map/sub | solution.py:84
  32.2 1.9 copy.54
  34.6 29.0 %fusion.9 = (f32[4,64,16,128]{3,1,0,2:T(8,128)S(1)}, f32[4,64,16,128]{3,1,0,2:T(8,128)}, f32[4,64,16,128]{3,1,0,2:T(8,128)S(1)}, f32[4,64,16,128]{3,1,0,2:T(8,128)S(1)}) fusion(f32[4,64]{1,0:T(4,128)S(1)} %reduce_window_sum.24, f32[128]{0:T(128)S(1)} %copy-done.27, f32[16,128]{1,0:T(8,128)S(1)} %get-tuple-element.398, f32[16,128]{1,0:T(8,128)S(1)} %get-tuple-element.459, ...), kind=kLoop, calls=%fused_computation.48 | loop fusion | flops 7340032 | bytes 8416256 | tf_op jit(solution)/shard_map/mul | solution.py:87
  69.2 32.3 %all-gather.2 = f32[128,128]{1,0:T(8,128)S(1)} all-gather(f32[16,128]{1,0:T(8,128)S(1)} %get-tuple-element.280), channel_id=4, replica_groups=mesh['sp'=8,'tp'=4] {'sp'}, dimensions={0}, use_global_device_ids=true | all-gather | bytes 73728 | tf_op jit(solution)/shard_map/all_gather | solution.py:15
  101.5 30.5 %all-gather.3 = f32[128,128]{1,0:T(8,128)S(1)} all-gather(f32[16,128]{1,0:T(8,128)S(1)} %get-tuple-element.281), channel_id=5, replica_groups=mesh['sp'=8,'tp'=4] {'sp'}, dimensions={0}, use_global_device_ids=true | all-gather | bytes 73728 | tf_op jit(solution)/shard_map/all_gather | solution.py:15
  134.5 2.0 bitcast_add_fusion.2
  138.3 2.7 fusion.36
  142.0 2.1 reshape.197
  145.9 2.9 copy.52
  148.8 4.6 multiply_subtract_fusion.9
  157.3 30.5 %all-gather = f32[128,128]{1,0:T(8,128)S(1)} all-gather(f32[16,128]{1,0:T(8,128)S(1)} %get-tuple-element.275), channel_id=2, replica_groups=mesh['sp'=8,'tp'=4] {'sp'}, dimensions={0}, use_global_device_ids=true | all-gather | bytes 73728 | tf_op jit(solution)/shard_map/all_gather | solution.py:15
  187.8 30.5 %all-gather.1 = f32[128,128]{1,0:T(8,128)S(1)} all-gather(f32[16,128]{1,0:T(8,128)S(1)} %get-tuple-element.276), channel_id=3, replica_groups=mesh['sp'=8,'tp'=4] {'sp'}, dimensions={0}, use_global_device_ids=true | all-gather | bytes 73728 | tf_op jit(solution)/shard_map/all_gather | solution.py:15
  220.0 1.9 bitcast_add_fusion.3
  223.3 2.7 fusion.39
  230.2 35.7 %all-reduce.2.cloned.1.call-done = bf16[256,2048]{1,0:T(8,128)(2,1)} async-done(((bf16[256,2048]{1,0:T(8,128)(2,1)}), bf16[256,2048]{1,0:T(8,128)(2,1)}) %all-reduce.2.cloned.1.call-update) | async-done | bytes 1048592 | tf_op jit(solution)/shard_map/psum | solution.py:174
  269.8 54.2 %all-gather.8.cloned.1.call-done = bf16[2048,1408]{1,0:T(8,128)(2,1)} async-done(((bf16[256,1408]{1,0:T(8,128)(2,1)}), bf16[2048,1408]{1,0:T(8,128)(2,1)}) %all-gather.8.cloned.1.call-update) | async-done | bytes 5767184 | tf_op jit(solution)/shard_map/all_gather | solution.py:184
  324.0 4.8 convolution_convert_fusion.1
  328.8 2.5 collective-permute-start
  332.6 83.8 %all-gather.10.cloned.1.call-done = bf16[2048,1408]{1,0:T(8,128)(2,1)} async-done(((bf16[256,1408]{1,0:T(8,128)(2,1)}), bf16[2048,1408]{1,0:T(8,128)(2,1)}) %all-gather.10.cloned.1.call-update) | async-done | bytes 5767184 | tf_op jit(solution)/shard_map/all_gather | solution.py:189
  416.4 5.3 convolution_convert_fusion
  423.0 86.4 %all-gather.12.cloned.1.call-done = bf16[1408,2048]{1,0:T(8,128)(2,1)} async-done(((bf16[1408,256]{1,0:T(8,128)(2,1)}), bf16[1408,2048]{1,0:T(8,128)(2,1)}) %all-gather.12.cloned.1.call-update) | async-done | bytes 5767184 | tf_op jit(solution)/shard_map/all_gather | solution.py:198
  509.3 7.7 %convolution_convert_fusion.3 = bf16[256,2048]{1,0:T(8,128)(2,1)} fusion(bf16[1408,2048]{1,0:T(8,128)(2,1)} %all-gather.12.cloned.1.call-done, f32[258,1408]{1,0:T(8,128)} %maximum_convert_fusion, bf16[256,1408]{1,0:T(8,128)(2,1)} %convolution_convert_fusion, f32[1408]{0:T(1024)S(1)} %get-tuple-element.348, f32[1408]{0:T(1024)S(1)} %get-tuple-element.349, ...), kind=kOutput, calls=%fused_computation.39 | convolution fusion | flops 1482686464 | bytes 11878912 | tf_op jit(solution)/shard_map/dot_general | solution.py:197
  517.1 23.1 %reduce-scatter.2.cloned.1.call-done = bf16[64,2048]{1,0:T(8,128)(2,1)} async-done(((bf16[256,2048]{1,0:T(8,128)(2,1)}), bf16[64,2048]{1,0:T(8,128)(2,1)}) %reduce-scatter.2.cloned.1.call-update) | async-done | bytes 262160 | tf_op jit(solution)/shard_map/reduce_scatter | solution.py:200
  (233 shorter events, 46.7 us)
Async XLA Ops:
  7.4 219.5 %copy-start = (bf16[256,2048]{1,0:T(8,128)(2,1)S(1)}, bf16[256,2048]{1,0:T(8,128)(2,1)}, u32[]{:S(2)}) copy-start(bf16[256,2048]{1,0:T(8,128)(2,1)} %param.33) | copy-start | bytes 3145732
  7.4 258.5 %all-reduce.2.cloned.1.call-start = ((), (), s32[]{:S(2)}) async-start(), calls=%async_computation.1 | async-start | bytes 2097152 | tf_op jit(solution)/shard_map/psum | solution.py:174
  9.7 5.3 copy-start.9
  11.7 3.4 copy-start.18
  11.7 3.4 copy-start.24
  11.7 3.5 copy-start.20
  11.7 3.5 copy-start.23
  11.7 3.4 copy-start.25
  15.2 14.3 %copy-start.8 = (f32[256,16,128]{0,2,1:T(8,128)S(1)}, f32[256,16,128]{0,2,1:T(8,128)}, u32[]{:S(2)}) copy-start(f32[256,16,128]{0,2,1:T(8,128)} %convolution_bitcast_fusion) | copy-start | bytes 6291460
  32.2 2.4 copy-start.27
  34.6 29.0 %copy-start.3 = (f32[256,16,128]{2,0,1:T(8,128)S(1)}, f32[256,16,128]{2,0,1:T(8,128)}, u32[]{:S(2)}) copy-start(f32[256,16,128]{2,0,1:T(8,128)} %copy.54) | copy-start | bytes 6291460
  63.7 4.7 copy-start.1
  69.2 32.3 %copy-start.17 = (f32[4,16,128]{2,1,0:T(8,128)}, f32[4,16,128]{2,1,0:T(8,128)S(1)}, u32[]{:S(2)}) copy-start(f32[4,16,128]{2,1,0:T(8,128)S(1)} %get-tuple-element.278) | copy-start | bytes 98308
  223.3 3.2 copy-start.13
  228.3 37.6 %copy-start.6 = (bf16[256,2048]{1,0:T(8,128)(2,1)S(1)}, bf16[256,2048]{1,0:T(8,128)(2,1)}, u32[]{:S(2)}) copy-start(bf16[256,2048]{1,0:T(8,128)(2,1)} %param.24) | copy-start | bytes 3145732
  228.3 95.7 %all-gather.8.cloned.1.call-start = ((), (), s32[]{:S(2)}) async-start(), calls=%async_computation.2 | async-start | bytes 6488064 | tf_op jit(solution)/shard_map/all_gather | solution.py:184
  228.9 187.5 %all-gather.10.cloned.1.call-start = ((), (), s32[]{:S(2)}) async-start(), calls=%async_computation.3 | async-start | bytes 6488064 | tf_op jit(solution)/shard_map/all_gather | solution.py:189
  229.5 279.9 %all-gather.12.cloned.1.call-start = ((), (), s32[]{:S(2)}) async-start(), calls=%async_computation.4 | async-start | bytes 6488064 | tf_op jit(solution)/shard_map/all_gather | solution.py:198
  230.1 310.1 %reduce-scatter.2.cloned.1.call-start = ((), (), s32[]{:S(2)}) async-start(), calls=%async_computation.5 | async-start | bytes 1310720 | tf_op jit(solution)/shard_map/reduce_scatter | solution.py:200
  230.2 38.1 %copy-start.21 = (f32[2048]{0:T(1024)S(1)}, f32[2048]{0:T(1024)}, u32[]{:S(2)}) copy-start(f32[2048]{0:T(1024)} %param.34) | copy-start | bytes 24580
  269.8 146.6 %copy-start.12 = (bf16[256,2048]{1,0:T(8,128)(2,1)S(1)}, bf16[256,2048]{1,0:T(8,128)(2,1)}, u32[]{:S(2)}) copy-start(bf16[256,2048]{1,0:T(8,128)(2,1)} %multiply_convert_fusion) | copy-start | bytes 3145732
  328.8 92.9 %collective-permute-start = (bf16[1,1408]{1,0:T(2,128)(2,1)S(1)}, bf16[1,1408]{1,0:T(2,128)(2,1)S(1)}, u32[]{:S(2)}, u32[]{:S(2)}) collective-permute-start(bf16[1,1408]{1,0:T(2,128)(2,1)S(1)} %get-tuple-element.436), channel_id=1, source_target_pairs={{0,4},{4,8},{8,12},{12,16},{16,20},{20,24},{24,28},{1,5},{5,9},{9,... | collective-permute-start | bytes 8456 | tf_op jit(solution)/shard_map/ppermute | solution.py:38
  331.3 90.4 %collective-permute-start.1 = (bf16[1,1408]{1,0:T(2,128)(2,1)S(1)}, bf16[1,1408]{1,0:T(2,128)(2,1)S(1)}, u32[]{:S(2)}, u32[]{:S(2)}) collective-permute-start(bf16[1,1408]{1,0:T(2,128)(2,1)S(1)} %get-tuple-element.437), channel_id=1, source_target_pairs={{4,0},{8,4},{12,8},{16,12},{20,16},{24,20},{28,24},{5,1},{9,5},{13... | collective-permute-start | bytes 8456 | tf_op jit(solution)/shard_map/ppermute | solution.py:40
  517.0 25.5 %copy-start.22 = (f32[2048]{0:T(1024)S(1)}, f32[2048]{0:T(1024)}, u32[]{:S(2)}) copy-start(f32[2048]{0:T(1024)} %param.39) | copy-start | bytes 24580
  (11 other events, 16.5 us)
Sparse Core Ops, SparseCore 0:
  228.4 37.4 all-reduce.1
  517.2 22.9 reduce-scatter.1
Sparse Core Ops, SparseCore 1:
  231.0 93.0 all-gather.7
  326.1 90.2 all-gather.9
  418.3 91.0 all-gather.11
where the time goes:
time: 560 us; the launch traced here: 552 us
  waiting for transfers between devices  285 us (51%)
  blocking collectives  124 us (22%)
  other arithmetic  73.8 us (13%)
  matrix products  31 us (6%)
  local copies, waits for them, and re-layouts  18.2 us (3%)
  between operations  16 us (3%)
    all_gather x4, blocking collectives, carried_in(): pieces = jax.tree.map(lambda part: lax.all_gather(part, axis), value)  124 us
    all_gather x1, waiting for transfers between devices, shards(): lax.all_gather(w_down, 'sp', axis=1, tiled=True)  86.4 us
    all_gather x1, waiting for transfers between devices, shards(): lax.all_gather(w_value, 'sp', axis=0, tiled=True)  83.8 us
    all_gather x1, waiting for transfers between devices, shards(): lax.all_gather(w_gate, 'sp', axis=0, tiled=True)  54.2 us
    psum x1, waiting for transfers between devices, shards(): lax.psum(jnp.dot(channels, w_out, preferred_element_type=jnp.float32).ast...  35.7 us
    mul x1, other arithmetic, local_pass(): jnp.exp(-pair_re * within) * jnp.cos(pair_im * within + phase_shift)  29 us
    reduce_scatter x1, waiting for transfers between devices, shards(): lax.psum_scatter(partials.astype(jnp.bfloat16), 'tp', scatter_dimension=0...  23.1 us
    sub x1, other arithmetic, local_pass(): driven = complex_mul(complex_mul(decays - identity_pair, rate_inv), inflow)  14.3 us
  transfers between devices with their start and end apart: 7, of which 5 were waited for; matrix products, arithmetic and copies ran while one was open for 3% of the time, Pallas kernels for 0%

commit v1 on v0

v1 whole, which is shorter than its diff:
```python
import functools
import math

import jax
import jax.numpy as jnp
from jax import lax
from jax.experimental import pallas as pl
from jax.experimental.pallas import tpu as pltpu
from jax.sharding import PartitionSpec as P

deep_alpha = 8.0**0.25
norm_eps = 1e-06
LANES = 128
SUB = 8
MESH = pl.DeviceIdType.MESH
F32 = jnp.float32
BF16 = jnp.bfloat16


def cmul(ar, ai, br, bi):
    return ar * br - ai * bi, ar * bi + ai * br


def sincos(angle):
    turns = jnp.floor(angle * (1.0 / (2.0 * math.pi)) + 0.5)
    rest = (angle - turns * 6.28125) - turns * (2.0 * math.pi - 6.28125)
    half = 0.5 * rest
    sq = half * half
    s = -1.0 / 39916800.0
    for c in (1.0 / 362880.0, -1.0 / 5040.0, 1.0 / 120.0, -1.0 / 6.0, 1.0):
        s = s * sq + c
    s = s * half
    c0 = 1.0 / 479001600.0
    for c in (-1.0 / 3628800.0, 1.0 / 40320.0, -1.0 / 720.0, 1.0 / 24.0, -0.5, 1.0):
        c0 = c0 * sq + c
    return 2.0 * s * c0, 1.0 - 2.0 * s * s


def normalize(pre, gain):
    mean = jnp.mean(pre, axis=-1, keepdims=True)
    cen = pre - mean
    spread = jnp.mean(cen * cen, axis=-1, keepdims=True)
    return cen * lax.rsqrt(spread + norm_eps) * gain


def gelu(x):
    return 0.5 * x * (1.0 + jnp.tanh(0.7978845608028654 * (x + 0.044715 * (x * x * x))))


def tile_ds(tile):
    return pl.ds(pl.multiple_of(tile * LANES, LANES), LANES)


def scan_kernel(half, width, u_ref, pace_ref, rows_ref, in_ref, sf_ref, sb_ref, pf_ref, pb_ref, tot_ref, flow, dec):
    positions = u_ref.shape[0]
    steps = positions // SUB
    tiles = rows_ref.shape[1] // LANES
    per_tile = LANES // half
    chans = u_ref.shape[1]
    row_group = lax.broadcasted_iota(jnp.int32, (chans, LANES), 0) // width
    lane_group = lax.broadcasted_iota(jnp.int32, (chans, LANES), 1) // half

    @pl.loop(0, tiles)
    def _(tile):
        lanes = tile_ds(tile)
        mask = row_group == lane_group + tile * per_tile
        for k in range(4):
            w = jnp.where(mask, in_ref[k].astype(F32), 0.0).astype(BF16)
            flow[k] = jnp.dot(u_ref[...], w, preferred_element_type=F32)
        step = rows_ref[0:1, lanes]
        damp = rows_ref[1:2, lanes]
        freq = rows_ref[2:3, lanes]
        ir = rows_ref[3:4, lanes]
        ii = rows_ref[4:5, lanes]
        one = jnp.ones((SUB, LANES), F32)
        zero = jnp.zeros((SUB, LANES), F32)

        def ahead(j, carry):
            sr, si, pr, pi = carry
            at = pl.ds(pl.multiple_of(j * SUB, SUB), SUB)
            delta = step * pace_ref[at, :]
            mag = jnp.exp(damp * delta)
            sn, cs = sincos(freq * delta)
            dr, di = mag * cs, mag * sn
            fr, fi = cmul(dr - 1.0, di, ir, ii)
            vr, vi = cmul(fr, fi, flow[0, at, :], flow[1, at, :])
            br, bi = cmul(fr, fi, flow[2, at, :], flow[3, at, :])
            flow[2, at, :] = br
            flow[3, at, :] = bi
            dec[0, at, :] = dr
            dec[1, at, :] = di
            sr, si = cmul(dr, di, sr, si)
            sr, si = sr + vr, si + vi
            pr, pi = cmul(dr, di, pr, pi)
            sf_ref[0, at, lanes] = sr
            sf_ref[1, at, lanes] = si
            pf_ref[0, at, lanes] = pr
            pf_ref[1, at, lanes] = pi
            return sr, si, pr, pi

        efr, efi, tr, ti = lax.fori_loop(0, steps, ahead, (zero, zero, one, zero), unroll=4)

        def behind(k, carry):
            sr, si, pr, pi = carry
            at = pl.ds(pl.multiple_of((steps - 1 - k) * SUB, SUB), SUB)
            dr, di = dec[0, at, :], dec[1, at, :]
            sr, si = cmul(dr, di, sr, si)
            sr, si = sr + flow[2, at, :], si + flow[3, at, :]
            pr, pi = cmul(dr, di, pr, pi)
            sb_ref[0, at, lanes] = sr
            sb_ref[1, at, lanes] = si
            pb_ref[0, at, lanes] = pr
            pb_ref[1, at, lanes] = pi
            return sr, si, pr, pi

        ebr, ebi, _, _ = lax.fori_loop(0, steps, behind, (zero, zero, one, zero), unroll=4)
        for k, v in enumerate((efr, efi, ebr, ebi, tr, ti)):
            tot_ref[k, :, lanes] = v


def join_chunks(tot, backward):
    n = tot.shape[1]
    off = 2 if backward else 0
    order = range(n - 1, -1, -1) if backward else range(n)
    cr = jnp.zeros_like(tot[0, 0])
    ci = jnp.zeros_like(cr)
    starts = [None] * n
    for s in order:
        starts[s] = (cr, ci)
        nr, ni = cmul(tot[4, s], tot[5, s], cr, ci)
        cr, ci = nr + tot[off, s], ni + tot[off + 1, s]
    return jnp.stack([a for a, _ in starts]), jnp.stack([b for _, b in starts]), cr, ci


def share_kernel(axis, n, x_ref, out_ref, got, send, recv):
    me = lax.axis_index(axis)
    barrier = pltpu.get_barrier_semaphore()
    for k in range(1, n):
        pl.semaphore_signal(barrier, inc=1, device_id={axis: lax.rem(me + k, n)}, device_id_type=MESH)
    pl.semaphore_wait(barrier, n - 1)
    copies = []
    for k in range(1, n):
        c = pltpu.make_async_remote_copy(
            src_ref=x_ref, dst_ref=got.at[k - 1], send_sem=send.at[k - 1], recv_sem=recv.at[k - 1],
            device_id={axis: lax.rem(me + k, n)}, device_id_type=MESH)
        c.start()
        copies.append(c)
    for c in copies:
        c.wait()
    out_ref[...] = got[...]


def share(x, axis, cid):
    n = lax.axis_size(axis)
    return pl.pallas_call(
        functools.partial(share_kernel, axis, n),
        out_shape=jax.ShapeDtypeStruct((n - 1,) + x.shape, x.dtype),
        in_specs=[pl.BlockSpec(memory_space=pltpu.VMEM)],
        out_specs=pl.BlockSpec(memory_space=pltpu.VMEM),
        scratch_shapes=[pltpu.VMEM((n - 1,) + x.shape, x.dtype),
                        pltpu.SemaphoreType.DMA((n - 1,)), pltpu.SemaphoreType.DMA((n - 1,))],
        compiler_params=pltpu.CompilerParams(collective_id=cid, has_side_effects=True),
        name="share_ends",
    )(x)


def readout_kernel(half, width, sf_ref, sb_ref, pf_ref, pb_ref, cin_ref, out_ref, u_ref, feed_ref, wo_ref, mixed_ref, acc):
    positions = u_ref.shape[0]
    steps = positions // SUB
    tiles = cin_ref.shape[2] // LANES
    per_tile = LANES // half
    chans = u_ref.shape[1]
    col_group = lax.broadcasted_iota(jnp.int32, (LANES, chans), 1) // width
    row_group = lax.broadcasted_iota(jnp.int32, (LANES, chans), 0) // half
    acc[...] = feed_ref[...] * u_ref[...].astype(F32)

    @pl.loop(0, tiles)
    def _(tile):
        lanes = tile_ds(tile)
        mask = col_group == row_group + tile * per_tile
        total = acc[...]
        for d, (s_ref, p_ref) in enumerate(((sf_ref, pf_ref), (sb_ref, pb_ref))):
            cr = jnp.broadcast_to(cin_ref[2 * d, :, lanes][None], (steps, SUB, LANES)).reshape(positions, LANES)
            ci = jnp.broadcast_to(cin_ref[2 * d + 1, :, lanes][None], (steps, SUB, LANES)).reshape(positions, LANES)
            ar, ai = cmul(p_ref[0, :, lanes], p_ref[1, :, lanes], cr, ci)
            for k, st in enumerate((ar + s_ref[0, :, lanes], ai + s_ref[1, :, lanes])):
                w = jnp.where(mask, out_ref[2 * d + k].astype(F32), 0.0).astype(BF16)
                total += jnp.dot(st.astype(BF16), w, preferred_element_type=F32)
        acc[...] = total

    channels = gelu(acc[...]).astype(BF16)
    row = lax.broadcasted_iota(jnp.int32, (positions, positions), 0)
    col = lax.broadcasted_iota(jnp.int32, (positions, positions), 1)
    pick = jnp.where(col == lax.rem(row, steps) * SUB + row // steps, 1.0, 0.0).astype(BF16)
    channels = jnp.dot(pick, channels, preferred_element_type=F32).astype(BF16)
    cols = wo_ref.shape[1]
    piece = min(512, cols)
    for c in range(cols // piece):
        at = slice(c * piece, (c + 1) * piece)
        mixed_ref[:, at] = jnp.dot(channels, wo_ref[:, at], preferred_element_type=F32).astype(BF16)


def settle_kernel(axis, n, spread, part_ref, res_ref, gain_ref, out_ref, got, whole, s1, r1, s2, r2):
    me = lax.axis_index(axis)
    rows = part_ref.shape[0] // n
    barrier = pltpu.get_barrier_semaphore()
    for k in range(1, n):
        pl.semaphore_signal(barrier, inc=1, device_id={axis: lax.rem(me + k, n)}, device_id_type=MESH)
    pl.semaphore_wait(barrier, n - 1)

    def span(who):
        return pl.ds(pl.multiple_of(who * rows, rows), rows)

    copies = []
    for k in range(1, n):
        peer = lax.rem(me + k, n)
        c = pltpu.make_async_remote_copy(
            src_ref=part_ref.at[span(peer)], dst_ref=got.at[k - 1], send_sem=s1.at[k - 1],
            recv_sem=r1.at[k - 1], device_id={axis: peer}, device_id_type=MESH)
        c.start()
        copies.append(c)
    total = part_ref[span(me), :].astype(F32)
    own = res_ref[span(me), :] if spread else res_ref[...]
    total = total + deep_alpha * own.astype(F32)
    for k in range(1, n):
        copies[k - 1].wait()
        total = total + got[k - 1].astype(F32)
    result = normalize(total, gain_ref[...]).astype(BF16)
    if not spread:
        out_ref[...] = result
        return
    whole[0] = result
    copies = []
    for k in range(1, n):
        c = pltpu.make_async_remote_copy(
            src_ref=whole.at[0], dst_ref=whole.at[k], send_sem=s2.at[k - 1], recv_sem=r2.at[k - 1],
            device_id={axis: lax.rem(me + k, n)}, device_id_type=MESH)
        c.start()
        copies.append(c)
    out_ref[span(me), :] = result
    for k in range(1, n):
        copies[k - 1].wait()
        out_ref[span(lax.rem(me + n - k, n)), :] = whole[k]


def settle(part, res, gain, axis, spread, cid):
    n = lax.axis_size(axis)
    rows = part.shape[0] // n
    width = part.shape[1]
    dma = pltpu.SemaphoreType.DMA((n - 1,))
    return pl.pallas_call(
        functools.partial(settle_kernel, axis, n, spread),
        out_shape=jax.ShapeDtypeStruct((part.shape[0] if spread else rows, width), BF16),
        in_specs=[pl.BlockSpec(memory_space=pltpu.VMEM)] * 3,
        out_specs=pl.BlockSpec(memory_space=pltpu.VMEM),
        scratch_shapes=[pltpu.VMEM((n - 1, rows, width), BF16), pltpu.VMEM((n, rows, width), BF16),
                        dma, dma, dma, dma],
        compiler_params=pltpu.CompilerParams(collective_id=cid, has_side_effects=True),
        cost_estimate=pl.CostEstimate(flops=2 * 10**9, bytes_accessed=part.size * 4, transcendentals=0),
        name="settle_spread" if spread else "settle_last",
    )(part, res, gain.reshape(1, -1))


def vmem(count):
    return [pl.BlockSpec(memory_space=pltpu.VMEM)] * count


def state_space(ssm_input, in_map, out_map, damping, log_step, frequency, pacing, feedthrough, w_out):
    positions, chans = ssm_input.shape
    groups, half = damping.shape
    width = chans // groups
    steps = positions // SUB
    flat = groups * half
    step = jnp.exp(log_step)[:, None] * jnp.ones((1, half), F32)
    modulus = damping * damping + frequency * frequency
    rows = jnp.stack([step, -damping, frequency, -damping / modulus, -frequency / modulus]).reshape(5, flat)
    u = ssm_input.reshape(SUB, steps, chans).transpose(1, 0, 2).reshape(positions, chans)
    pace = pacing.reshape(SUB, steps).T.reshape(positions, 1) * jnp.ones((1, LANES), F32)
    reps = LANES // half
    in_cols = in_map.reshape(2, chans, 2, half).transpose(0, 2, 1, 3).reshape(4, chans, half)
    in_cols = jnp.tile(in_cols, (1, 1, reps))
    out_rows = out_map.reshape(2, chans, 2, half).transpose(0, 2, 3, 1).reshape(4, half, chans)
    out_rows = jnp.tile(out_rows, (1, reps, 1))
    big = jax.ShapeDtypeStruct((2, positions, flat), F32)
    sf, sb, pf, pb, tot = pl.pallas_call(
        functools.partial(scan_kernel, half, width),
        out_shape=(big, big, big, big, jax.ShapeDtypeStruct((6, SUB, flat), F32)),
        in_specs=vmem(4),
        out_specs=tuple(vmem(5)),
        scratch_shapes=[pltpu.VMEM((4, positions, LANES), F32), pltpu.VMEM((2, positions, LANES), F32)],
        cost_estimate=pl.CostEstimate(flops=4 * 10**9, bytes_accessed=10**7, transcendentals=0),
        name="scan_local",
    )(u, pace, rows, in_cols)
    fr, fi, fer, fei = join_chunks(tot, False)
    br, bi, ber, bei = join_chunks(tot, True)
    ones, zeros = jnp.ones((flat,), F32), jnp.zeros((flat,), F32)
    pre = [(ones, zeros)]
    suf = [(ones, zeros)]
    for s in range(SUB):
        pre.append(cmul(*pre[-1], tot[4, s], tot[5, s]))
        suf.append(cmul(*suf[-1], tot[4, SUB - 1 - s], tot[5, SUB - 1 - s]))
    mine = jnp.stack([fer, fei, ber, bei, pre[-1][0], pre[-1][1]]).reshape(6, flat // LANES, LANES)
    n = lax.axis_size("sp")
    me = lax.axis_index("sp")
    got = share(mine, "sp", 3).reshape(n - 1, 6, flat)
    cfr, cfi, cbr, cbi = zeros, zeros, zeros, zeros
    for k in range(n - 1, 0, -1):
        far = got[k - 1]
        nr, ni = cmul(far[4], far[5], cfr, cfi)
        use = me - k >= 0
        cfr, cfi = jnp.where(use, nr + far[0], cfr), jnp.where(use, ni + far[1], cfi)
        far = got[n - k - 1]
        nr, ni = cmul(far[4], far[5], cbr, cbi)
        use = me + k < n
        cbr, cbi = jnp.where(use, nr + far[2], cbr), jnp.where(use, ni + far[3], cbi)
    prr = jnp.stack([p[0] for p in pre[:-1]])
    pri = jnp.stack([p[1] for p in pre[:-1]])
    sur = jnp.stack([p[0] for p in suf[:-1]][::-1])
    sui = jnp.stack([p[1] for p in suf[:-1]][::-1])
    ar, ai = cmul(prr, pri, cfr, cfi)
    er, ei = cmul(sur, sui, cbr, cbi)
    cin = jnp.stack([fr + ar, fi + ai, br + er, bi + ei])
    return pl.pallas_call(
        functools.partial(readout_kernel, half, width),
        out_shape=jax.ShapeDtypeStruct((positions, w_out.shape[1]), BF16),
        in_specs=vmem(9),
        out_specs=pl.BlockSpec(memory_space=pltpu.VMEM),
        scratch_shapes=[pltpu.VMEM((positions, chans), F32)],
        cost_estimate=pl.CostEstimate(flops=4 * 10**9, bytes_accessed=10**7, transcendentals=0),
        name="read_states",
    )(sf, sb, pf, pb, cin, out_rows, u, feedthrough.reshape(1, -1), w_out)


def edges(gated):
    n = lax.axis_size("sp")
    before = lax.ppermute(gated[-1:], "sp", [(i, i + 1) for i in range(n - 1)])
    after = lax.ppermute(gated[:1], "sp", [(i + 1, i) for i in range(n - 1)])
    return jnp.concatenate([before, gated, after], axis=0)


def shards(residual, ssm_input, in_map, out_map, damping, log_step, frequency, pacing, feedthrough,
           w_out, gain_mix, w_gate, w_value, conv_taps, w_down, gain_ffn):
    positions = ssm_input.shape[0]
    own_rows = positions // lax.axis_size("tp")
    gate_all = lax.all_gather(w_gate, "sp", axis=0, tiled=True)
    value_all = lax.all_gather(w_value, "sp", axis=0, tiled=True)
    down_all = lax.all_gather(w_down, "sp", axis=1, tiled=True)
    partial = state_space(ssm_input, in_map, out_map, damping, log_step, frequency, pacing, feedthrough, w_out)
    rows = settle(partial, residual, gain_mix, "tp", True, 4)
    gated = jnp.dot(rows, gate_all, preferred_element_type=F32).astype(BF16)
    padded = edges(gated).astype(F32)
    values = jnp.dot(rows, value_all, preferred_element_type=F32).astype(BF16).astype(F32)
    smoothed = conv_taps[0] * padded[:-2] + conv_taps[1] * padded[1:-1] + conv_taps[2] * padded[2:]
    hidden = (jax.nn.gelu(smoothed) * values).astype(BF16)
    parts = jnp.dot(hidden, down_all, preferred_element_type=F32).astype(BF16)
    kept = lax.dynamic_slice_in_dim(rows, lax.axis_index("tp") * own_rows, own_rows, 0)
    return settle(parts, kept, gain_ffn, "tp", False, 5)


def solution(mesh):
    in_specs = (
        P("sp", None), P("sp", "tp"), P(None, "tp", None, None), P(None, "tp", None, None),
        P("tp", None), P("tp"), P("tp", None), P("sp"), P("tp"), P("tp", None), P(),
        P("sp", "tp"), P("sp", "tp"), P(None, "tp"), P("tp", "sp"), P(),
    )
    return jax.shard_map(shards, mesh=mesh, in_specs=in_specs, out_specs=P(("sp", "tp"), None), check_vma=False)
```

time: 560 us -> 329 us (0.59); the launches traced: 552 us -> 328 us
  blocking collectives: 124 us -> 0 us
  waiting for transfers between devices: 285 us -> 203 us
  Pallas kernels: 0 us -> 77.2 us
  other arithmetic: 73.8 us -> 4.06 us
  matrix products: 31 us -> 14 us
  local copies, waits for them, and re-layouts: 18.2 us -> 12.1 us
    all_gather x4 -> x0, blocking collectives: 124 us -> none  [carried_in(): pieces = jax.tree.map(lambda part: lax.all_gather(part, axis), value)]
    pallas_call x0 -> x5, Pallas kernels: none -> 77.2 us  [the longest x2 43.3 us: settle(): pl.pallas_call(functools.partial(settle_kernel, axis, n, spread), out_sha...]
    psum x1 -> x0, waiting for transfers between devices: 35.7 us -> none  [shards(): lax.psum(jnp.dot(channels, w_out, preferred_element_type=jnp.float32).ast...]
    mul x1 -> x0, other arithmetic: 29 us -> none  [local_pass(): jnp.exp(-pair_re * within) * jnp.cos(pair_im * within + phase_shift)]
    all_gather x3, waiting for transfers between devices: 224 us -> 197 us  [the longest x1 93.4 us: shards(): down_all = lax.all_gather(w_down, 'sp', axis=1, tiled=True)]
    sub x30 -> x5, other arithmetic: 26.4 us -> 2.69 us  [cmul(): return (ar * br - ai * bi, ar * bi + ai * br)]
    reduce_scatter x1 -> x0, waiting for transfers between devices: 23.1 us -> none  [shards(): lax.psum_scatter(partials.astype(jnp.bfloat16), 'tp', scatter_dimension=0...]
    dot_general x10 -> x2, matrix products: 31 us -> 14 us  [the longest x1 9.23 us: shards(): parts = jnp.dot(hidden, down_all, preferred_element_type=F32).astype(BF16)]
  transfers between devices with their start and end apart: 7 -> 5, of which waited for: 5 -> 4; matrix products, arithmetic and copies ran while one was open for 3% -> 6% of each run, Pallas kernels for 0% -> 19%
where the time goes in v1:
time: 329 us; the launch traced here: 328 us
  waiting for transfers between devices  203 us (62%)
  Pallas kernels  77.2 us (23%)
  matrix products  14 us (4%)
  between operations  13.5 us (4%)
  local copies, waits for them, and re-layouts  12.1 us (4%)
  other arithmetic  4.06 us (1%)
  starting transfers between devices  3.99 us (1%)
    all_gather x1, waiting for transfers between devices, shards(): down_all = lax.all_gather(w_down, 'sp', axis=1, tiled=True)  93.4 us
    all_gather x1, waiting for transfers between devices, shards(): value_all = lax.all_gather(w_value, 'sp', axis=0, tiled=True)  79.5 us
    pallas_call x2, Pallas kernels, settle(): pl.pallas_call(functools.partial(settle_kernel, axis, n, spread), out_sha...  43.3 us
    all_gather x1, waiting for transfers between devices, shards(): gate_all = lax.all_gather(w_gate, 'sp', axis=0, tiled=True)  23.9 us
    pallas_call x1, Pallas kernels, share(): pl.pallas_call(functools.partial(share_kernel, axis, n), out_shape=jax.Sh...  14.6 us
    pallas_call x1, Pallas kernels, state_space(): pl.pallas_call(functools.partial(scan_kernel, half, width), out_shape=(bi...  11.1 us
    dot_general x1, matrix products, shards(): parts = jnp.dot(hidden, down_all, preferred_element_type=F32).astype(BF16)  9.23 us
    pallas_call x1, Pallas kernels, state_space(): pl.pallas_call(functools.partial(readout_kernel, half, width), out_shape=...  8.25 us
  transfers between devices with their start and end apart: 5, of which 4 were waited for; matrix products, arithmetic and copies ran while one was open for 6% of the time, Pallas kernels for 19%

profile of v1, /device:TPU:0, one launch (start us, length us, event | category | flops | bytes accessed | tf_op | source)
XLA Modules:
  0.0 328.0 jit_solution(11177906860005143842)
XLA Ops:
  7.3 0.7 all-gather.6.cloned.1.call-update
  9.3 0.7 copy.28
  10.3 0.8 copy.25.in_ref
  12.1 0.8 mul.4436.pace_ref
  12.8 11.1 %scan_local.1 = (f32[2,256,1024]{2,1,0:T(8,128)}, f32[2,256,1024]{2,1,0:T(8,128)}, f32[2,256,1024]{2,1,0:T(8,128)}, f32[2,256,1024]{2,1,0:T(8,128)}, f32[6,8,1024]{2,1,0:T(8,128)}) custom-call(bf16[256,256]{1,0:T(8,128)(2,1)} %bitcast.464, f32[256,128]{1,0:T(8,128)} %mul.4436.pace_ref, f32[5,1024]{1,0:T(8,128)} %stack.44.rows_ref, ...), custom_call_target="tpu_custom_call" | custom-call | flops 4000000000 | bytes 10000000 | tf_op jit(solution)/shard_map/scan_local/pallas_call | solution.py:285
  23.9 1.3 fusion.91
  25.3 1.3 multiply_subtract_fusion
  26.6 1.2 fusion.90
  27.9 1.3 multiply_subtract_fusion.12
  30.2 14.6 %share_ends.1 = f32[7,6,8,128]{3,2,1,0:T(8,128)} custom-call(f32[6,8,128]{2,1,0:T(8,128)} %copy-done.6), custom_call_target="tpu_custom_call" | custom-call | tf_op jit(solution)/shard_map/share_ends/pallas_call | solution.py:155
  46.6 0.7 tile.24
  47.3 8.2 %read_states.1.part_ref = bf16[256,2048]{1,0:T(8,128)(2,1)} custom-call(f32[2,256,1024]{2,1,0:T(8,128)} %get-tuple-element.10.sf_ref, f32[2,256,1024]{2,1,0:T(8,128)} %get-tuple-element.11.sb_ref, f32[2,256,1024]{2,1,0:T(8,128)} %get-tuple-element.12.pf_ref, f32[2,256,1024]{2,1,0:T(8,128)} %get-tuple-element.13.pb_ref, ...), custom_call_target="tpu_custom_call" | custom-call | flops 4000000000 | bytes 10000000 | tf_op jit(solution)/shard_map/read_states/pallas_call | solution.py:323
  55.6 27.7 %settle_spread.1 = bf16[256,2048]{1,0:T(8,128)(2,1)} custom-call(bf16[256,2048]{1,0:T(8,128)(2,1)} %read_states.1.part_ref, bf16[256,2048]{1,0:T(8,128)(2,1)} %res_ref.1, f32[1,2048]{1,0:T(1,128)} %bitcast.535), custom_call_target="tpu_custom_call" | custom-call | flops 2000000000 | bytes 2097152 | tf_op jit(solution)/shard_map/settle_spread/pallas_call | solution.py:251
  83.2 1.7 constant_dynamic-slice_fusion.res_ref
  84.9 23.9 %all-gather.4.cloned.1.call-done = bf16[2048,1408]{1,0:T(8,128)(2,1)} async-done(((bf16[256,1408]{1,0:T(8,128)(2,1)}), bf16[2048,1408]{1,0:T(8,128)(2,1)}) %all-gather.4.cloned.1.call-update) | async-done | bytes 5767184 | tf_op jit(solution)/shard_map/all_gather | solution.py:345
  108.8 4.8 %convolution_convert_fusion.1 = bf16[256,1408]{1,0:T(8,128)(2,1)S(1)} fusion(bf16[256,2048]{1,0:T(8,128)(2,1)} %settle_spread.1, bf16[2048,1408]{1,0:T(8,128)(2,1)} %all-gather.4.cloned.1.call-done), kind=kOutput, calls=%fused_computation.4 | convolution fusion | flops 1476755456 | bytes 7536640 | tf_op jit(solution)/shard_map/dot_general | solution.py:350
  113.6 2.6 collective-permute-start
  116.2 1.3 collective-permute-start.1
  117.6 4.3 %collective-permute-done.1 = bf16[1,1408]{1,0:T(2,128)(2,1)S(1)} collective-permute-done((bf16[1,1408]{1,0:T(2,128)(2,1)S(1)}, bf16[1,1408]{1,0:T(2,128)(2,1)S(1)}, u32[]{:S(2)}, u32[]{:S(2)}) %collective-permute-start.1) | collective-permute-done | bytes 2848 | tf_op jit(solution)/shard_map/ppermute | solution.py:337
  122.0 79.5 %all-gather.6.cloned.1.call-done = bf16[2048,1408]{1,0:T(8,128)(2,1)} async-done(((bf16[256,1408]{1,0:T(8,128)(2,1)}), bf16[2048,1408]{1,0:T(8,128)(2,1)}) %all-gather.6.cloned.1.call-update) | async-done | bytes 5767184 | tf_op jit(solution)/shard_map/all_gather | solution.py:346
  201.5 93.4 %all-gather.8.cloned.1.call-done = bf16[1408,2048]{1,0:T(8,128)(2,1)} async-done(((bf16[1408,256]{1,0:T(8,128)(2,1)}), bf16[1408,2048]{1,0:T(8,128)(2,1)}) %all-gather.8.cloned.1.call-update) | async-done | bytes 5767184 | tf_op jit(solution)/shard_map/all_gather | solution.py:347
  294.9 9.2 %convolution_convert_fusion.2.part_ref = bf16[256,2048]{1,0:T(8,128)(2,1)} fusion(bf16[1408,2048]{1,0:T(8,128)(2,1)} %all-gather.8.cloned.1.call-done, bf16[256,2048]{1,0:T(8,128)(2,1)S(1)} %copy-done.5, bf16[2048,1408]{1,0:T(8,128)(2,1)} %all-gather.6.cloned.1.call-done, f32[258,1408]{1,0:T(8,128)S(1)} %maximum_convert_fusion, ...), kind=kOutput, calls=%fused_computation.5 | convolution fusion | flops 2959441920 | bytes 17981440 | tf_op jit(solution)/shard_map/dot_general | solution.py:355
  304.2 15.6 %settle_last.1 = bf16[64,2048]{1,0:T(8,128)(2,1)} custom-call(bf16[256,2048]{1,0:T(8,128)(2,1)} %convolution_convert_fusion.2.part_ref, bf16[64,2048]{1,0:T(8,128)(2,1)} %constant_dynamic-slice_fusion.res_ref, f32[1,2048]{1,0:T(1,128)} %bitcast.536), custom_call_target="tpu_custom_call" | custom-call | flops 2000000000 | bytes 2097152 | tf_op jit(solution)/shard_map/settle_last/pallas_call | solution.py:251
  319.8 1.7 copy.35
  (86 shorter events, 6.1 us)
Async XLA Ops:
  6.5 2.2 copy-start.7
  6.5 2.3 copy-start.9
  6.5 2.6 copy-start.11
  6.5 2.7 copy-start.4
  6.5 3.5 %copy-start.2 = (bf16[2,16,16,128]{3,2,1,0:T(8,128)(2,1)S(1)}, bf16[2,16,16,128]{3,2,1,0:T(8,128)(2,1)}, u32[]{:S(2)}) copy-start(bf16[2,16,16,128]{3,2,1,0:T(8,128)(2,1)} %param.18) | copy-start | bytes 393220
  6.5 102.3 %all-gather.4.cloned.1.call-start = ((), (), s32[]{:S(2)}) async-start(), calls=%async_computation | async-start | bytes 6488064 | tf_op jit(solution)/shard_map/all_gather | solution.py:345
  7.3 194.3 %all-gather.6.cloned.1.call-start = ((), (), s32[]{:S(2)}) async-start(), calls=%async_computation.1 | async-start | bytes 6488064 | tf_op jit(solution)/shard_map/all_gather | solution.py:346
  8.0 3.1 copy-start.10
  8.0 286.9 %all-gather.8.cloned.1.call-start = ((), (), s32[]{:S(2)}) async-start(), calls=%async_computation.2 | async-start | bytes 6488064 | tf_op jit(solution)/shard_map/all_gather | solution.py:347
  23.9 5.4 %copy-start = (f32[6,8,1024]{2,1,0:T(8,128)S(1)}, f32[6,8,1024]{2,1,0:T(8,128)}, u32[]{:S(2)}) copy-start(f32[6,8,1024]{2,1,0:T(8,128)} %get-tuple-element.14) | copy-start | bytes 589828
  23.9 21.0 %copy-start.3 = (bf16[2,16,16,128]{3,2,1,0:T(8,128)(2,1)S(1)}, bf16[2,16,16,128]{3,2,1,0:T(8,128)(2,1)}, u32[]{:S(2)}) copy-start(bf16[2,16,16,128]{3,2,1,0:T(8,128)(2,1)} %param.19) | copy-start | bytes 393220
  29.6 0.6 copy-start.6
  44.8 0.9 copy-start.1
  84.9 32.6 %copy-start.8 = (f32[3,1408]{1,0:T(4,128)S(1)}, f32[3,1408]{1,0:T(4,128)}, u32[]{:S(2)}) copy-start(f32[3,1408]{1,0:T(4,128)} %param.29) | copy-start | bytes 50692
  113.6 181.4 %copy-start.5 = (bf16[256,2048]{1,0:T(8,128)(2,1)S(1)}, bf16[256,2048]{1,0:T(8,128)(2,1)}, u32[]{:S(2)}) copy-start(bf16[256,2048]{1,0:T(8,128)(2,1)} %settle_spread.1) | copy-start | bytes 3145732
  113.6 4.0 %collective-permute-start = (bf16[1,1408]{1,0:T(2,128)(2,1)S(1)}, bf16[1,1408]{1,0:T(2,128)(2,1)S(1)}, u32[]{:S(2)}, u32[]{:S(2)}) collective-permute-start(bf16[1,1408]{1,0:T(2,128)(2,1)S(1)} %get-tuple-element.115), channel_id=1, source_target_pairs={{0,4},{4,8},{8,12},{12,16},{16,20},{20,24},{24,28},{1,5},{5,9},{9,... | collective-permute-start | bytes 8456 | tf_op jit(solution)/shard_map/ppermute | solution.py:336
  116.2 5.7 %collective-permute-start.1 = (bf16[1,1408]{1,0:T(2,128)(2,1)S(1)}, bf16[1,1408]{1,0:T(2,128)(2,1)S(1)}, u32[]{:S(2)}, u32[]{:S(2)}) collective-permute-start(bf16[1,1408]{1,0:T(2,128)(2,1)S(1)} %get-tuple-element.116), channel_id=1, source_target_pairs={{4,0},{8,4},{12,8},{16,12},{20,16},{24,20},{28,24},{5,1},{9,5},{13... | collective-permute-start | bytes 8456 | tf_op jit(solution)/shard_map/ppermute | solution.py:337
Sparse Core Ops, SparseCore 0:
  9.5 99.2 all-gather.3
  111.0 90.5 all-gather.5
  203.6 91.2 all-gather.7

commit v2 on v1

--- a/solution.py
+++ b/solution.py
@@ -118,52 +118,6 @@
             tot_ref[k, :, lanes] = v
 
 
-def join_chunks(tot, backward):
-    n = tot.shape[1]
-    off = 2 if backward else 0
-    order = range(n - 1, -1, -1) if backward else range(n)
-    cr = jnp.zeros_like(tot[0, 0])
-    ci = jnp.zeros_like(cr)
-    starts = [None] * n
-    for s in order:
-        starts[s] = (cr, ci)
-        nr, ni = cmul(tot[4, s], tot[5, s], cr, ci)
-        cr, ci = nr + tot[off, s], ni + tot[off + 1, s]
-    return jnp.stack([a for a, _ in starts]), jnp.stack([b for _, b in starts]), cr, ci
-
-
-def share_kernel(axis, n, x_ref, out_ref, got, send, recv):
-    me = lax.axis_index(axis)
-    barrier = pltpu.get_barrier_semaphore()
-    for k in range(1, n):
-        pl.semaphore_signal(barrier, inc=1, device_id={axis: lax.rem(me + k, n)}, device_id_type=MESH)
-    pl.semaphore_wait(barrier, n - 1)
-    copies = []
-    for k in range(1, n):
-        c = pltpu.make_async_remote_copy(
-            src_ref=x_ref, dst_ref=got.at[k - 1], send_sem=send.at[k - 1], recv_sem=recv.at[k - 1],
-            device_id={axis: lax.rem(me + k, n)}, device_id_type=MESH)
-        c.start()
-        copies.append(c)
-    for c in copies:
-        c.wait()
-    out_ref[...] = got[...]
-
-
-def share(x, axis, cid):
-    n = lax.axis_size(axis)
-    return pl.pallas_call(
-        functools.partial(share_kernel, axis, n),
-        out_shape=jax.ShapeDtypeStruct((n - 1,) + x.shape, x.dtype),
-        in_specs=[pl.BlockSpec(memory_space=pltpu.VMEM)],
-        out_specs=pl.BlockSpec(memory_space=pltpu.VMEM),
-        scratch_shapes=[pltpu.VMEM((n - 1,) + x.shape, x.dtype),
-                        pltpu.SemaphoreType.DMA((n - 1,)), pltpu.SemaphoreType.DMA((n - 1,))],
-        compiler_params=pltpu.CompilerParams(collective_id=cid, has_side_effects=True),
-        name="share_ends",
-    )(x)
-
-
 def readout_kernel(half, width, sf_ref, sb_ref, pf_ref, pb_ref, cin_ref, out_ref, u_ref, feed_ref, wo_ref, mixed_ref, acc):
     positions = u_ref.shape[0]
     steps = positions // SUB
@@ -200,13 +154,18 @@
         mixed_ref[:, at] = jnp.dot(channels, wo_ref[:, at], preferred_element_type=F32).astype(BF16)
 
 
-def settle_kernel(axis, n, spread, part_ref, res_ref, gain_ref, out_ref, got, whole, s1, r1, s2, r2):
+def settle_kernel(axis, n, spread, part_ref, *refs):
     me = lax.axis_index(axis)
-    rows = part_ref.shape[0] // n
     barrier = pltpu.get_barrier_semaphore()
     for k in range(1, n):
         pl.semaphore_signal(barrier, inc=1, device_id={axis: lax.rem(me + k, n)}, device_id_type=MESH)
     pl.semaphore_wait(barrier, n - 1)
+    settle_body(axis, n, spread, part_ref, *refs)
+
+
+def settle_body(axis, n, spread, part_ref, res_ref, gain_ref, out_ref, got, whole, s1, r1, s2, r2):
+    me = lax.axis_index(axis)
+    rows = part_ref.shape[0] // n
 
     def span(who):
         return pl.ds(pl.multiple_of(who * rows, rows), rows)
@@ -265,12 +224,231 @@
     return [pl.BlockSpec(memory_space=pltpu.VMEM)] * count
 
 
-def state_space(ssm_input, in_map, out_map, damping, log_step, frequency, pacing, feedthrough, w_out):
+def carry_ends(tot, mine):
+    chunks = tot.shape[1]
+    zero = jnp.zeros((1, tot.shape[2]), F32)
+
+    def row(k, s):
+        return tot[k, s:s + 1, :]
+
+    fr, fi, br, bi = zero, zero, zero, zero
+    pr, pi = zero + 1.0, zero
+    for s in range(chunks):
+        t = chunks - 1 - s
+        nr, ni = cmul(row(4, s), row(5, s), fr, fi)
+        fr, fi = nr + row(0, s), ni + row(1, s)
+        nr, ni = cmul(row(4, t), row(5, t), br, bi)
+        br, bi = nr + row(2, t), ni + row(3, t)
+        pr, pi = cmul(row(4, s), row(5, s), pr, pi)
+    for k, v in enumerate((fr, fi, br, bi, pr, pi, zero, zero)):
+        mine[k:k + 1, :] = v
+
+
+def carry_starts(tot, got, cin, me, n):
+    chunks = tot.shape[1]
+    zero = jnp.zeros((1, tot.shape[2]), F32)
+
+    def far(i, carry):
+        fr, fi, br, bi = carry
+        k = n - 1 - i
+        early, late = got.at[k - 1], got.at[n - k - 1]
+        nr, ni = cmul(early[4:5, :], early[5:6, :], fr, fi)
+        use = me - k >= 0
+        fr, fi = jnp.where(use, nr + early[0:1, :], fr), jnp.where(use, ni + early[1:2, :], fi)
+        nr, ni = cmul(late[4:5, :], late[5:6, :], br, bi)
+        use = me + k < n
+        br, bi = jnp.where(use, nr + late[2:3, :], br), jnp.where(use, ni + late[3:4, :], bi)
+        return fr, fi, br, bi
+
+    fr, fi, br, bi = lax.fori_loop(0, n - 1, far, (zero, zero, zero, zero))
+    for s in range(chunks):
+        t = chunks - 1 - s
+        cin[0, s:s + 1, :] = fr
+        cin[1, s:s + 1, :] = fi
+        cin[2, t:t + 1, :] = br
+        cin[3, t:t + 1, :] = bi
+        nr, ni = cmul(tot[4, s:s + 1, :], tot[5, s:s + 1, :], fr, fi)
+        fr, fi = nr + tot[0, s:s + 1, :], ni + tot[1, s:s + 1, :]
+        nr, ni = cmul(tot[4, t:t + 1, :], tot[5, t:t + 1, :], br, bi)
+        br, bi = nr + tot[2, t:t + 1, :], ni + tot[3, t:t + 1, :]
+
+
+class Gather:
+    def __init__(self, n, sources, targets, parts, pair_first, send, recv, local):
+        self.n, self.outer = n, n // 2
+        me = lax.axis_index("sp")
+        self.me, self.z, self.y = me, me // 2, lax.rem(me, 2)
+        self.send, self.recv, self.local = send, recv, local
+        self.sources, self.targets = sources, targets
+        self.items = []
+        for w, src in enumerate(sources):
+            rows = src.shape[0] // parts
+            for p in range(parts):
+                self.items.append((w, pl.ds(p * rows, rows), (w, p) in pair_first))
+
+    def copy(self, i, slot, block, dest, own=False):
+        w, rows, _ = self.items[i]
+        dst = self.targets[w].at[block, rows]
+        src = self.sources[w].at[rows] if own else dst
+        return pltpu.make_async_remote_copy(
+            src_ref=src, dst_ref=dst, send_sem=self.send.at[i, slot], recv_sem=self.recv.at[i, slot],
+            device_id={"sp": dest}, device_id_type=MESH)
+
+    def slot(self, left, r, second):
+        return r - 1 + (self.outer - 1) * (int(left) + 2 * int(second))
+
+    def at(self, z, other=False):
+        return z * 2 + (1 - self.y if other else self.y)
+
+    def begin(self, first, last):
+        o, z = self.outer, self.z
+        for i in range(first, last):
+            self.copy(i, 4 * (o - 1), self.me, self.at(z, True), own=True).start()
+
+            @pl.when(z + 1 < o)
+            def _():
+                self.copy(i, self.slot(False, 1, False), self.me, self.at(z + 1), own=True).start()
+
+            @pl.when(z >= 1)
+            def _():
+                self.copy(i, self.slot(True, 1, False), self.me, self.at(z - 1), own=True).start()
+
+    def begin_local(self):
+        for w, src in enumerate(self.sources):
+            pltpu.make_async_copy(src, self.targets[w].at[self.me], self.local.at[w]).start()
+
+    def finish(self):
+        o, z = self.outer, self.z
+        count = len(self.items)
+        pair_own = 4 * (o - 1)
+        for i in range(count):
+            if self.items[i][2]:
+                other = self.at(z, True)
+                self.copy(i, pair_own, other, other).wait_recv()
+
+                @pl.when(z + 1 < o)
+                def _():
+                    self.copy(i, self.slot(False, 1, True), other, self.at(z + 1)).start()
+
+                @pl.when(z >= 1)
+                def _():
+                    self.copy(i, self.slot(True, 1, True), other, self.at(z - 1)).start()
+
+        @pl.loop(1, o)
+        def _(r):
+            for i in range(count):
+                pair_first = self.items[i][2]
+                for left in (False, True):
+                    far = z + r if left else z - r
+                    to = z - 1 if left else z + 1
+                    has = far < o if left else far >= 0
+                    on = to >= 0 if left else to < o
+
+                    @pl.when(has)
+                    def _():
+                        self.copy(i, self.slot(left, r, False), self.at(far), self.me).wait_recv()
+
+                        @pl.when(on)
+                        def _():
+                            self.copy(i, self.slot(left, r + 1, False), self.at(far), self.at(to)).start()
+
+                        if pair_first:
+                            self.copy(i, self.slot(left, r, True), self.at(far, True), self.me).wait_recv()
+
+                            @pl.when(on)
+                            def _():
+                                self.copy(i, self.slot(left, r + 1, True), self.at(far, True), self.at(to)).start()
+                        else:
+                            self.copy(i, self.slot(left, r, True), self.at(far), self.at(z, True)).start()
+
+        for i in range(count):
+            if not self.items[i][2]:
+                self.copy(i, pair_own, self.at(z, True), self.me).wait_recv()
+            self.copy(i, pair_own, self.me, self.at(z, True), own=True).wait_send()
+        for w, src in enumerate(self.sources):
+            pltpu.make_async_copy(src, self.targets[w].at[self.me], self.local.at[w]).wait()
+
+        @pl.loop(1, o)
+        def _(r):
+            for i in range(count):
+                pair_first = self.items[i][2]
+                for left in (False, True):
+                    far = z + r if left else z - r
+                    to = z - 1 if left else z + 1
+                    sent = z + r - 1 if left else z - r + 1
+                    has = far < o if left else far >= 0
+                    did = jnp.logical_and(sent < o, to >= 0) if left else jnp.logical_and(sent >= 0, to < o)
+
+                    @pl.when(did)
+                    def _():
+                        self.copy(i, self.slot(left, r, False), self.at(sent), self.at(to)).wait_send()
+                        if pair_first:
+                            self.copy(i, self.slot(left, r, True), self.at(sent, True), self.at(to)).wait_send()
+
+                    if not pair_first:
+                        @pl.when(has)
+                        def _():
+                            c = self.copy(i, self.slot(left, r, True), self.at(far, True), self.at(z, True))
+                            c.wait_recv()
+                            c.wait_send()
+
+
+def front_kernel(half, width, n, n_tp, parts, pair_first, early,
+                 u_ref, pace_ref, rows_ref, in_ref, out_ref, feed_ref, wo_ref, res_ref, gain_ref,
+                 gate_ref, value_ref, down_ref,
+                 whole_ref, gate_all, value_all, down_all,
+                 flow, dec, sf, sb, pf, pb, tot, mine, far, cin, acc, part, got, whole,
+                 s0, r0, s1, r1, s2, r2, gsend, grecv, glocal):
+    me = lax.axis_index("sp")
+    tp = lax.axis_index("tp")
+    barrier = pltpu.get_barrier_semaphore()
+
+    @pl.loop(1, n)
+    def _(k):
+        pl.semaphore_signal(barrier, inc=1, device_id={"sp": lax.rem(me + k, n)}, device_id_type=MESH)
+
+    for k in range(1, n_tp):
+        pl.semaphore_signal(barrier, inc=1, device_id={"tp": lax.rem(tp + k, n_tp)}, device_id_type=MESH)
+    pl.semaphore_wait(barrier, n - 1 + n_tp - 1)
+
+    weights = Gather(n, (gate_ref, value_ref, down_ref), (gate_all, value_all, down_all), parts, pair_first,
+                     gsend, grecv, glocal)
+    total = len(weights.items)
+    weights.begin(0, early)
+    scan_kernel(half, width, u_ref, pace_ref, rows_ref, in_ref, sf, sb, pf, pb, tot, flow, dec)
+    carry_ends(tot, mine)
+
+    def shared(k):
+        return pltpu.make_async_remote_copy(
+            src_ref=mine, dst_ref=far.at[k - 1], send_sem=s0.at[k - 1], recv_sem=r0.at[k - 1],
+            device_id={"sp": lax.rem(me + k, n)}, device_id_type=MESH)
+
+    @pl.loop(1, n)
+    def _(k):
+        shared(k).start()
+
+    weights.begin(early, total)
+    weights.begin_local()
+
+    @pl.loop(1, n)
+    def _(k):
+        shared(k).wait()
+
+    carry_starts(tot, far, cin, me, n)
+    readout_kernel(half, width, sf, sb, pf, pb, cin, out_ref, u_ref, feed_ref, wo_ref, part, acc)
+    settle_body("tp", n_tp, True, part, res_ref, gain_ref, whole_ref, got, whole, s1, r1, s2, r2)
+    weights.finish()
+
+
+def front(residual, ssm_input, in_map, out_map, damping, log_step, frequency, pacing, feedthrough, w_out,
+          gain_mix, w_gate, w_value, w_down):
     positions, chans = ssm_input.shape
     groups, half = damping.shape
     width = chans // groups
     steps = positions // SUB
     flat = groups * half
+    model = residual.shape[1]
+    n, n_tp = lax.axis_size("sp"), lax.axis_size("tp")
     step = jnp.exp(log_step)[:, None] * jnp.ones((1, half), F32)
     modulus = damping * damping + frequency * frequency
     rows = jnp.stack([step, -damping, frequency, -damping / modulus, -frequency / modulus]).reshape(5, flat)
@@ -281,54 +459,36 @@
     in_cols = jnp.tile(in_cols, (1, 1, reps))
     out_rows = out_map.reshape(2, chans, 2, half).transpose(0, 2, 3, 1).reshape(4, half, chans)
     out_rows = jnp.tile(out_rows, (1, reps, 1))
-    big = jax.ShapeDtypeStruct((2, positions, flat), F32)
-    sf, sb, pf, pb, tot = pl.pallas_call(
-        functools.partial(scan_kernel, half, width),
-        out_shape=(big, big, big, big, jax.ShapeDtypeStruct((6, SUB, flat), F32)),
-        in_specs=vmem(4),
-        out_specs=tuple(vmem(5)),
-        scratch_shapes=[pltpu.VMEM((4, positions, LANES), F32), pltpu.VMEM((2, positions, LANES), F32)],
+    parts = 2 if n <= 16 else 1
+    pair_first = ((2, 0),) if parts == 2 else ()
+    items = 3 * parts
+    slots = 4 * (n // 2 - 1) + 1
+    dma = pltpu.SemaphoreType.DMA
+    own = positions // n_tp
+    big = pltpu.VMEM((2, positions, flat), F32)
+    anywhere = pl.BlockSpec(memory_space=pl.ANY)
+    shards_of = (w_gate, w_value, w_down)
+    return pl.pallas_call(
+        functools.partial(front_kernel, half, width, n, n_tp, parts, pair_first, min(2, items)),
+        out_shape=(jax.ShapeDtypeStruct((positions, model), BF16),)
+        + tuple(jax.ShapeDtypeStruct((n,) + w.shape, BF16) for w in shards_of),
+        in_specs=vmem(9) + [anywhere] * 3,
+        out_specs=tuple(vmem(1) + [anywhere] * 3),
+        scratch_shapes=[
+            pltpu.VMEM((4, positions, LANES), F32), pltpu.VMEM((2, positions, LANES), F32),
+            big, big, big, big,
+            pltpu.VMEM((6, SUB, flat), F32), pltpu.VMEM((8, flat), F32), pltpu.VMEM((n - 1, 8, flat), F32),
+            pltpu.VMEM((4, SUB, flat), F32), pltpu.VMEM((positions, chans), F32),
+            pltpu.VMEM((positions, model), BF16),
+            pltpu.VMEM((n_tp - 1, own, model), BF16), pltpu.VMEM((n_tp, own, model), BF16),
+            dma((n - 1,)), dma((n - 1,)), dma((n_tp - 1,)), dma((n_tp - 1,)), dma((n_tp - 1,)), dma((n_tp - 1,)),
+            dma((items, slots)), dma((items, slots)), dma((3,)),
+        ],
+        compiler_params=pltpu.CompilerParams(collective_id=3, has_side_effects=True),
         cost_estimate=pl.CostEstimate(flops=4 * 10**9, bytes_accessed=10**7, transcendentals=0),
-        name="scan_local",
-    )(u, pace, rows, in_cols)
-    fr, fi, fer, fei = join_chunks(tot, False)
-    br, bi, ber, bei = join_chunks(tot, True)
-    ones, zeros = jnp.ones((flat,), F32), jnp.zeros((flat,), F32)
-    pre = [(ones, zeros)]
-    suf = [(ones, zeros)]
-    for s in range(SUB):
-        pre.append(cmul(*pre[-1], tot[4, s], tot[5, s]))
-        suf.append(cmul(*suf[-1], tot[4, SUB - 1 - s], tot[5, SUB - 1 - s]))
-    mine = jnp.stack([fer, fei, ber, bei, pre[-1][0], pre[-1][1]]).reshape(6, flat // LANES, LANES)
-    n = lax.axis_size("sp")
-    me = lax.axis_index("sp")
-    got = share(mine, "sp", 3).reshape(n - 1, 6, flat)
-    cfr, cfi, cbr, cbi = zeros, zeros, zeros, zeros
-    for k in range(n - 1, 0, -1):
-        far = got[k - 1]
-        nr, ni = cmul(far[4], far[5], cfr, cfi)
-        use = me - k >= 0
-        cfr, cfi = jnp.where(use, nr + far[0], cfr), jnp.where(use, ni + far[1], cfi)
-        far = got[n - k - 1]
-        nr, ni = cmul(far[4], far[5], cbr, cbi)
-        use = me + k < n
-        cbr, cbi = jnp.where(use, nr + far[2], cbr), jnp.where(use, ni + far[3], cbi)
-    prr = jnp.stack([p[0] for p in pre[:-1]])
-    pri = jnp.stack([p[1] for p in pre[:-1]])
-    sur = jnp.stack([p[0] for p in suf[:-1]][::-1])
-    sui = jnp.stack([p[1] for p in suf[:-1]][::-1])
-    ar, ai = cmul(prr, pri, cfr, cfi)
-    er, ei = cmul(sur, sui, cbr, cbi)
-    cin = jnp.stack([fr + ar, fi + ai, br + er, bi + ei])
-    return pl.pallas_call(
-        functools.partial(readout_kernel, half, width),
-        out_shape=jax.ShapeDtypeStruct((positions, w_out.shape[1]), BF16),
-        in_specs=vmem(9),
-        out_specs=pl.BlockSpec(memory_space=pltpu.VMEM),
-        scratch_shapes=[pltpu.VMEM((positions, chans), F32)],
-        cost_estimate=pl.CostEstimate(flops=4 * 10**9, bytes_accessed=10**7, transcendentals=0),
-        name="read_states",
-    )(sf, sb, pf, pb, cin, out_rows, u, feedthrough.reshape(1, -1), w_out)
+        name="front",
+    )(u, pace, rows, in_cols, out_rows, feedthrough.reshape(1, -1), w_out, residual, gain_mix.reshape(1, -1),
+      w_gate, w_value, w_down)
 
 
 def edges(gated):
@@ -342,17 +502,18 @@
            w_out, gain_mix, w_gate, w_value, conv_taps, w_down, gain_ffn):
     positions = ssm_input.shape[0]
     own_rows = positions // lax.axis_size("tp")
-    gate_all = lax.all_gather(w_gate, "sp", axis=0, tiled=True)
-    value_all = lax.all_gather(w_value, "sp", axis=0, tiled=True)
-    down_all = lax.all_gather(w_down, "sp", axis=1, tiled=True)
-    partial = state_space(ssm_input, in_map, out_map, damping, log_step, frequency, pacing, feedthrough, w_out)
-    rows = settle(partial, residual, gain_mix, "tp", True, 4)
+    rows, gate_all, value_all, down_all = front(
+        residual, ssm_input, in_map, out_map, damping, log_step, frequency, pacing, feedthrough, w_out,
+        gain_mix, w_gate, w_value, w_down)
+    gate_all = gate_all.reshape(-1, w_gate.shape[1])
+    value_all = value_all.reshape(-1, w_value.shape[1])
     gated = jnp.dot(rows, gate_all, preferred_element_type=F32).astype(BF16)
     padded = edges(gated).astype(F32)
     values = jnp.dot(rows, value_all, preferred_element_type=F32).astype(BF16).astype(F32)
     smoothed = conv_taps[0] * padded[:-2] + conv_taps[1] * padded[1:-1] + conv_taps[2] * padded[2:]
     hidden = (jax.nn.gelu(smoothed) * values).astype(BF16)
-    parts = jnp.dot(hidden, down_all, preferred_element_type=F32).astype(BF16)
+    parts = jnp.einsum("th,nhc->tnc", hidden, down_all, preferred_element_type=F32).astype(BF16)
+    parts = parts.reshape(positions, -1)
     kept = lax.dynamic_slice_in_dim(rows, lax.axis_index("tp") * own_rows, own_rows, 0)
     return settle(parts, kept, gain_ffn, "tp", False, 5)
 

time: 329 us -> 238 us (0.72)
  waiting for transfers between devices: 203 us -> 2.48 us
  Pallas kernels: 77.2 us -> 202 us
  between operations: 13.5 us -> 0.15 us
    all_gather x3 -> x0, waiting for transfers between devices: 197 us -> none  [the longest x1 93.4 us: shards(): down_all = lax.all_gather(w_down, 'sp', axis=1, tiled=True)]
    pallas_call x3 -> x1, Pallas kernels: 33.9 us -> 187 us  [front(): pl.pallas_call(functools.partial(front_kernel, half, width, n, n_tp, part...]
    pallas_call x2 -> x1, Pallas kernels: 43.3 us -> 15.8 us  [settle(): pl.pallas_call(functools.partial(settle_kernel, axis, n, spread), out_sha...]
  transfers between devices with their start and end apart: 5 -> 2, of which waited for: 4 -> 1; matrix products, arithmetic and copies ran while one was open for 6% -> 1% of each run, Pallas kernels for 19% -> 0%
where the time goes in v2:
time: 238 us; the launch traced here: 237 us
  Pallas kernels  202 us (85%)
  matrix products  13.4 us (6%)
  local copies, waits for them, and re-layouts  12.1 us (5%)
  starting transfers between devices  5.68 us (2%)
  waiting for transfers between devices  2.48 us (1%)
    pallas_call x1, Pallas kernels, front(): pl.pallas_call(functools.partial(front_kernel, half, width, n, n_tp, part...  187 us
    pallas_call x1, Pallas kernels, settle(): pl.pallas_call(functools.partial(settle_kernel, axis, n, spread), out_sha...  15.8 us
    dot_general x1, matrix products, shards(): jnp.einsum('th,nhc->tnc', hidden, down_all, preferred_element_type=F32)  8.62 us
    dot_general x1, matrix products, shards(): gated = jnp.dot(rows, gate_all, preferred_element_type=F32).astype(BF16)  4.77 us
  transfers between devices with their start and end apart: 2, of which 1 were waited for; matrix products, arithmetic and copies ran while one was open for 1% of the time, Pallas kernels for 0%

profile of v2, /device:TPU:0, one launch (start us, length us, event | category | flops | bytes accessed | tf_op | source)
XLA Modules:
  0.0 237.0 jit_solution(1641240958084367801)
XLA Ops:
  0.0 0.8 stack.23
  0.8 0.7 negate_divide_fusion
  1.8 0.7 exp.3
  2.6 1.0 reshape.60
  3.6 0.1 copy.28
  3.8 0.8 copy.30.in_ref
  4.7 0.1 reshape.61
  4.8 0.1 copy.29
  5.1 0.1 mul.75
  5.2 0.7 copy.36
  5.9 0.6 stack.26.rows_ref
  6.6 0.7 tile.24
  7.3 0.7 mul.76.pace_ref
  8.0 186.6 %front.1 = (bf16[256,2048]{1,0:T(8,128)(2,1)}, bf16[8,256,1408]{2,1,0:T(8,128)(2,1)}, bf16[8,256,1408]{2,1,0:T(8,128)(2,1)}, bf16[8,1408,256]{2,1,0:T(8,128)(2,1)}) custom-call(bf16[256,256]{1,0:T(8,128)(2,1)} %bitcast.40, f32[256,128]{1,0:T(8,128)} %mul.76.pace_ref, f32[5,1024]{1,0:T(8,128)} %stack.26.rows_ref, bf16[4,256,128]{2,1,0:T(8,128)(2,1)} %copy.30.in_ref, ...), custom_call_target="tpu_custom_call" | custom-call | flops 4000000000 | bytes 10000000 | tf_op jit(solution)/shard_map/front/pallas_call | solution.py:471
  194.6 4.8 %convolution_convert_fusion.1 = bf16[256,1408]{1,0:T(8,128)(2,1)S(1)} fusion(bf16[256,2048]{1,0:T(8,128)(2,1)} %get-tuple-element.9, bf16[2048,1408]{1,0:T(8,128)(2,1)} %bitcast.46), kind=kOutput, calls=%fused_computation.4 | convolution fusion | flops 1476755456 | bytes 7536640 | tf_op jit(solution)/shard_map/dot_general | solution.py:510
  199.4 4.4 %collective-permute-start = (bf16[1,1408]{1,0:T(2,128)(2,1)S(1)}, bf16[1,1408]{1,0:T(2,128)(2,1)S(1)}, u32[]{:S(2)}, u32[]{:S(2)}) collective-permute-start(bf16[1,1408]{1,0:T(2,128)(2,1)S(1)} %get-tuple-element.16), channel_id=1, source_target_pairs={{0,4},{4,8},{8,12},{12,16},{16,20},{20,24},{24,28},{1,5},{5,9},{9,... | collective-permute-start | bytes 8456 | tf_op jit(solution)/shard_map/ppermute | solution.py:496
  203.8 1.3 collective-permute-start.1
  205.1 1.7 constant_dynamic-slice_fusion.refs_0_
  206.8 2.5 %collective-permute-done.1 = bf16[1,1408]{1,0:T(2,128)(2,1)S(1)} collective-permute-done((bf16[1,1408]{1,0:T(2,128)(2,1)S(1)}, bf16[1,1408]{1,0:T(2,128)(2,1)S(1)}, u32[]{:S(2)}, u32[]{:S(2)}) %collective-permute-start.1) | collective-permute-done | bytes 2848 | tf_op jit(solution)/shard_map/ppermute | solution.py:497
  209.3 0.2 maximum_convert_fusion
  209.5 8.6 %convolution_convert_fusion.2 = bf16[256,8,256]{0,2,1:T(8,128)(2,1)S(1)} fusion(bf16[8,1408,256]{2,1,0:T(8,128)(2,1)} %get-tuple-element.12, bf16[256,2048]{1,0:T(8,128)(2,1)} %get-tuple-element.9, bf16[2048,1408]{1,0:T(8,128)(2,1)} %bitcast.45, f32[258,1408]{1,0:T(8,128)S(1)} %maximum_convert_fusion, f32[1408]{0:T(1024)S(1)} %get-tuple-element.14, ...), kind=kOutput, calls=%fused_computation.7 | convolution fusion | flops 2959441920 | bytes 17981440 | tf_op jit(solution)/shard_map/th,nhc->tnc/dot_general | solution.py:515
  218.1 1.4 copy.34.part_ref
  219.5 15.8 %settle_last.1 = bf16[64,2048]{1,0:T(8,128)(2,1)} custom-call(bf16[256,2048]{1,0:T(8,128)(2,1)} %copy.34.part_ref, bf16[64,2048]{1,0:T(8,128)(2,1)} %constant_dynamic-slice_fusion.refs_0_, f32[1,2048]{1,0:T(1,128)} %bitcast.43), custom_call_target="tpu_custom_call" | custom-call | flops 2000000000 | bytes 2097152 | tf_op jit(solution)/shard_map/settle_last/pallas_call | solution.py:210
  235.4 1.7 copy.38
  (19 shorter events, 0.6 us)
Async XLA Ops:
  0.0 4.7 %copy-start = (bf16[2,16,16,128]{3,2,1,0:T(8,128)(2,1)S(1)}, bf16[2,16,16,128]{3,2,1,0:T(8,128)(2,1)}, u32[]{:S(2)}) copy-start(bf16[2,16,16,128]{3,2,1,0:T(8,128)(2,1)} %param.19) | copy-start | bytes 393220
  0.0 4.9 %copy-start.3 = (f32[256]{0:T(256)S(1)}, f32[256]{0:T(256)}, u32[]{:S(2)}) copy-start(f32[256]{0:T(256)} %param.23) | copy-start | bytes 3076
  0.0 5.2 %copy-start.1 = (bf16[256,256]{1,0:T(8,128)(2,1)S(1)}, bf16[256,256]{1,0:T(8,128)(2,1)}, u32[]{:S(2)}) copy-start(bf16[256,256]{1,0:T(8,128)(2,1)} %param.17) | copy-start | bytes 393220
  194.6 12.2 %copy-start.2 = (f32[3,1408]{1,0:T(4,128)S(1)}, f32[3,1408]{1,0:T(4,128)}, u32[]{:S(2)}) copy-start(f32[3,1408]{1,0:T(4,128)} %param.29) | copy-start | bytes 50692
  199.4 7.4 %collective-permute-start = (bf16[1,1408]{1,0:T(2,128)(2,1)S(1)}, bf16[1,1408]{1,0:T(2,128)(2,1)S(1)}, u32[]{:S(2)}, u32[]{:S(2)}) collective-permute-start(bf16[1,1408]{1,0:T(2,128)(2,1)S(1)} %get-tuple-element.16), channel_id=1, source_target_pairs={{0,4},{4,8},{8,12},{12,16},{16,20},{20,24},{24,28},{1,5},{5,9},{9,... | collective-permute-start | bytes 8456 | tf_op jit(solution)/shard_map/ppermute | solution.py:496
  203.8 5.5 %collective-permute-start.1 = (bf16[1,1408]{1,0:T(2,128)(2,1)S(1)}, bf16[1,1408]{1,0:T(2,128)(2,1)S(1)}, u32[]{:S(2)}, u32[]{:S(2)}) collective-permute-start(bf16[1,1408]{1,0:T(2,128)(2,1)S(1)} %get-tuple-element.17), channel_id=1, source_target_pairs={{4,0},{8,4},{12,8},{16,12},{20,16},{24,20},{28,24},{5,1},{9,5},{13... | collective-permute-start | bytes 8456 | tf_op jit(solution)/shard_map/ppermute | solution.py:497

commit v3 on v2

--- a/solution.py
+++ b/solution.py
@@ -154,72 +154,6 @@
         mixed_ref[:, at] = jnp.dot(channels, wo_ref[:, at], preferred_element_type=F32).astype(BF16)
 
 
-def settle_kernel(axis, n, spread, part_ref, *refs):
-    me = lax.axis_index(axis)
-    barrier = pltpu.get_barrier_semaphore()
-    for k in range(1, n):
-        pl.semaphore_signal(barrier, inc=1, device_id={axis: lax.rem(me + k, n)}, device_id_type=MESH)
-    pl.semaphore_wait(barrier, n - 1)
-    settle_body(axis, n, spread, part_ref, *refs)
-
-
-def settle_body(axis, n, spread, part_ref, res_ref, gain_ref, out_ref, got, whole, s1, r1, s2, r2):
-    me = lax.axis_index(axis)
-    rows = part_ref.shape[0] // n
-
-    def span(who):
-        return pl.ds(pl.multiple_of(who * rows, rows), rows)
-
-    copies = []
-    for k in range(1, n):
-        peer = lax.rem(me + k, n)
-        c = pltpu.make_async_remote_copy(
-            src_ref=part_ref.at[span(peer)], dst_ref=got.at[k - 1], send_sem=s1.at[k - 1],
-            recv_sem=r1.at[k - 1], device_id={axis: peer}, device_id_type=MESH)
-        c.start()
-        copies.append(c)
-    total = part_ref[span(me), :].astype(F32)
-    own = res_ref[span(me), :] if spread else res_ref[...]
-    total = total + deep_alpha * own.astype(F32)
-    for k in range(1, n):
-        copies[k - 1].wait()
-        total = total + got[k - 1].astype(F32)
-    result = normalize(total, gain_ref[...]).astype(BF16)
-    if not spread:
-        out_ref[...] = result
-        return
-    whole[0] = result
-    copies = []
-    for k in range(1, n):
-        c = pltpu.make_async_remote_copy(
-            src_ref=whole.at[0], dst_ref=whole.at[k], send_sem=s2.at[k - 1], recv_sem=r2.at[k - 1],
-            device_id={axis: lax.rem(me + k, n)}, device_id_type=MESH)
-        c.start()
-        copies.append(c)
-    out_ref[span(me), :] = result
-    for k in range(1, n):
-        copies[k - 1].wait()
-        out_ref[span(lax.rem(me + n - k, n)), :] = whole[k]
-
-
-def settle(part, res, gain, axis, spread, cid):
-    n = lax.axis_size(axis)
-    rows = part.shape[0] // n
-    width = part.shape[1]
-    dma = pltpu.SemaphoreType.DMA((n - 1,))
-    return pl.pallas_call(
-        functools.partial(settle_kernel, axis, n, spread),
-        out_shape=jax.ShapeDtypeStruct((part.shape[0] if spread else rows, width), BF16),
-        in_specs=[pl.BlockSpec(memory_space=pltpu.VMEM)] * 3,
-        out_specs=pl.BlockSpec(memory_space=pltpu.VMEM),
-        scratch_shapes=[pltpu.VMEM((n - 1, rows, width), BF16), pltpu.VMEM((n, rows, width), BF16),
-                        dma, dma, dma, dma],
-        compiler_params=pltpu.CompilerParams(collective_id=cid, has_side_effects=True),
-        cost_estimate=pl.CostEstimate(flops=2 * 10**9, bytes_accessed=part.size * 4, transcendentals=0),
-        name="settle_spread" if spread else "settle_last",
-    )(part, res, gain.reshape(1, -1))
-
-
 def vmem(count):
     return [pl.BlockSpec(memory_space=pltpu.VMEM)] * count
 
@@ -274,70 +208,88 @@
 
 
 class Gather:
-    def __init__(self, n, sources, targets, parts, pair_first, send, recv, local):
-        self.n, self.outer = n, n // 2
+    def __init__(self, n, half_of, sources, targets, pair_first, send, recv, local, csend, crecv):
+        self.n, self.m, self.outer = n, n // 2, n // 4
         me = lax.axis_index("sp")
-        self.me, self.z, self.y = me, me // 2, lax.rem(me, 2)
-        self.send, self.recv, self.local = send, recv, local
-        self.sources, self.targets = sources, targets
-        self.items = []
-        for w, src in enumerate(sources):
-            rows = src.shape[0] // parts
-            for p in range(parts):
-                self.items.append((w, pl.ds(p * rows, rows), (w, p) in pair_first))
+        self.me, self.side = me, me // self.m
+        place = lax.rem(me, self.m)
+        self.z, self.y = place // 2, lax.rem(place, 2)
+        self.mate = lax.rem(me + self.m, n)
+        self.send, self.recv, self.local, self.csend, self.crecv = send, recv, local, csend, crecv
+        self.sources, self.targets, self.half_of = sources, targets, half_of
+        self.items = [(w, kind) for kind in range(2) for w in range(len(sources))]
+        self.pair_first = pair_first
+
+    def cut(self, w, side):
+        dim, size = self.half_of[w]
+        start = pl.multiple_of(side * (self.sources[w].shape[dim] - size), LANES)
+        at = pl.ds(start, size)
+        return self.sources[w].at[at] if dim == 0 else self.sources[w].at[:, at]
+
+    def device(self, z, other=False):
+        return self.side * self.m + z * 2 + (1 - self.y if other else self.y)
+
+    def block(self, i, z, other=False):
+        side = 1 - self.side if self.items[i][1] else self.side
+        return side * self.m + z * 2 + (1 - self.y if other else self.y)
 
     def copy(self, i, slot, block, dest, own=False):
-        w, rows, _ = self.items[i]
-        dst = self.targets[w].at[block, rows]
-        src = self.sources[w].at[rows] if own else dst
+        w, kind = self.items[i]
+        dst = self.targets[w].at[block]
+        src = self.cut(w, self.side) if own and kind == 0 else dst
         return pltpu.make_async_remote_copy(
             src_ref=src, dst_ref=dst, send_sem=self.send.at[i, slot], recv_sem=self.recv.at[i, slot],
             device_id={"sp": dest}, device_id_type=MESH)
 
+    def cross(self, w, block):
+        return pltpu.make_async_remote_copy(
+            src_ref=self.cut(w, 1 - self.side), dst_ref=self.targets[w].at[block], send_sem=self.csend.at[w],
+            recv_sem=self.crecv.at[w], device_id={"sp": self.mate}, device_id_type=MESH)
+
     def slot(self, left, r, second):
         return r - 1 + (self.outer - 1) * (int(left) + 2 * int(second))
 
-    def at(self, z, other=False):
-        return z * 2 + (1 - self.y if other else self.y)
-
-    def begin(self, first, last):
+    @property
+    def pair_own(self):
+        return 4 * (self.outer - 1)
+
+    def begin(self, i):
         o, z = self.outer, self.z
-        for i in range(first, last):
-            self.copy(i, 4 * (o - 1), self.me, self.at(z, True), own=True).start()
-
-            @pl.when(z + 1 < o)
-            def _():
-                self.copy(i, self.slot(False, 1, False), self.me, self.at(z + 1), own=True).start()
-
-            @pl.when(z >= 1)
-            def _():
-                self.copy(i, self.slot(True, 1, False), self.me, self.at(z - 1), own=True).start()
+        mine = self.block(i, z)
+        self.copy(i, self.pair_own, mine, self.device(z, True), own=True).start()
+
+        @pl.when(z + 1 < o)
+        def _():
+            self.copy(i, self.slot(False, 1, False), mine, self.device(z + 1), own=True).start()
+
+        @pl.when(z >= 1)
+        def _():
+            self.copy(i, self.slot(True, 1, False), mine, self.device(z - 1), own=True).start()
 
     def begin_local(self):
-        for w, src in enumerate(self.sources):
-            pltpu.make_async_copy(src, self.targets[w].at[self.me], self.local.at[w]).start()
-
-    def finish(self):
+        for w in range(len(self.sources)):
+            pltpu.make_async_copy(self.cut(w, self.side), self.targets[w].at[self.me], self.local.at[w]).start()
+
+    def second(self, i):
         o, z = self.outer, self.z
-        count = len(self.items)
-        pair_own = 4 * (o - 1)
-        for i in range(count):
-            if self.items[i][2]:
-                other = self.at(z, True)
-                self.copy(i, pair_own, other, other).wait_recv()
-
-                @pl.when(z + 1 < o)
-                def _():
-                    self.copy(i, self.slot(False, 1, True), other, self.at(z + 1)).start()
-
-                @pl.when(z >= 1)
-                def _():
-                    self.copy(i, self.slot(True, 1, True), other, self.at(z - 1)).start()
+        other = self.block(i, z, True)
+        self.copy(i, self.pair_own, other, self.me).wait_recv()
+
+        @pl.when(z + 1 < o)
+        def _():
+            self.copy(i, self.slot(False, 1, True), other, self.device(z + 1)).start()
+
+        @pl.when(z >= 1)
+        def _():
+            self.copy(i, self.slot(True, 1, True), other, self.device(z - 1)).start()
+
+    def pump(self, which):
+        o, z = self.outer, self.z
 
         @pl.loop(1, o)
         def _(r):
-            for i in range(count):
-                pair_first = self.items[i][2]
+            for i in which:
+                pair_first = i in self.pair_first
                 for left in (False, True):
                     far = z + r if left else z - r
                     to = z - 1 if left else z + 1
@@ -346,32 +298,37 @@
 
                     @pl.when(has)
                     def _():
-                        self.copy(i, self.slot(left, r, False), self.at(far), self.me).wait_recv()
+                        self.copy(i, self.slot(left, r, False), self.block(i, far), self.me).wait_recv()
 
                         @pl.when(on)
                         def _():
-                            self.copy(i, self.slot(left, r + 1, False), self.at(far), self.at(to)).start()
+                            self.copy(i, self.slot(left, r + 1, False), self.block(i, far), self.device(to)).start()
 
                         if pair_first:
-                            self.copy(i, self.slot(left, r, True), self.at(far, True), self.me).wait_recv()
+                            self.copy(i, self.slot(left, r, True), self.block(i, far, True), self.me).wait_recv()
 
                             @pl.when(on)
                             def _():
-                                self.copy(i, self.slot(left, r + 1, True), self.at(far, True), self.at(to)).start()
+                                self.copy(i, self.slot(left, r + 1, True), self.block(i, far, True),
+                                          self.device(to)).start()
                         else:
-                            self.copy(i, self.slot(left, r, True), self.at(far), self.at(z, True)).start()
-
+                            self.copy(i, self.slot(left, r, True), self.block(i, far), self.device(z, True)).start()
+
+    def finish(self):
+        o, z = self.outer, self.z
+        count = len(self.items)
         for i in range(count):
-            if not self.items[i][2]:
-                self.copy(i, pair_own, self.at(z, True), self.me).wait_recv()
-            self.copy(i, pair_own, self.me, self.at(z, True), own=True).wait_send()
-        for w, src in enumerate(self.sources):
-            pltpu.make_async_copy(src, self.targets[w].at[self.me], self.local.at[w]).wait()
+            if i not in self.pair_first:
+                self.copy(i, self.pair_own, self.block(i, z, True), self.me).wait_recv()
+            self.copy(i, self.pair_own, self.block(i, z), self.device(z, True), own=True).wait_send()
+        for w in range(len(self.sources)):
+            pltpu.make_async_copy(self.cut(w, self.side), self.targets[w].at[self.me], self.local.at[w]).wait()
+            self.cross(w, self.me).wait_send()
 
         @pl.loop(1, o)
         def _(r):
             for i in range(count):
-                pair_first = self.items[i][2]
+                pair_first = i in self.pair_first
                 for left in (False, True):
                     far = z + r if left else z - r
                     to = z - 1 if left else z + 1
@@ -381,24 +338,116 @@
 
                     @pl.when(did)
                     def _():
-                        self.copy(i, self.slot(left, r, False), self.at(sent), self.at(to)).wait_send()
+                        self.copy(i, self.slot(left, r, False), self.block(i, sent), self.device(to)).wait_send()
                         if pair_first:
-                            self.copy(i, self.slot(left, r, True), self.at(sent, True), self.at(to)).wait_send()
+                            self.copy(i, self.slot(left, r, True), self.block(i, sent, True),
+                                      self.device(to)).wait_send()
 
                     if not pair_first:
                         @pl.when(has)
                         def _():
-                            c = self.copy(i, self.slot(left, r, True), self.at(far, True), self.at(z, True))
+                            c = self.copy(i, self.slot(left, r, True), self.block(i, far, True), self.device(z, True))
                             c.wait_recv()
                             c.wait_send()
 
 
-def front_kernel(half, width, n, n_tp, parts, pair_first, early,
+def to_peers(axis, n, src, slots, send, recv):
+    me = lax.axis_index(axis)
+    copies = []
+    for k in range(1, n):
+        c = pltpu.make_async_remote_copy(
+            src_ref=src(lax.rem(me + k, n)), dst_ref=slots(k), send_sem=send.at[k - 1], recv_sem=recv.at[k - 1],
+            device_id={axis: lax.rem(me + k, n)}, device_id_type=MESH)
+        c.start()
+        copies.append(c)
+    return copies
+
+
+def span(who, rows, base=0):
+    return pl.ds(pl.multiple_of(base + who * rows, rows), rows)
+
+
+def mix_rows(n, mate, side, part, res_ref, gain_ref, rows_ref, got, whole, theirs, s1, r1, s2, r2, s3, r3, sm, rm):
+    me = lax.axis_index("tp")
+    positions = part.shape[0]
+    rows = positions // n
+    copies = to_peers("tp", n, lambda peer: part.at[span(peer, rows)], lambda k: got.at[k - 1], s1, r1)
+    total = part[span(me, rows), :].astype(F32) + deep_alpha * res_ref[span(me, rows), :].astype(F32)
+    for k in range(1, n):
+        copies[k - 1].wait()
+        total = total + got[k - 1].astype(F32)
+    result = normalize(total, gain_ref[...]).astype(BF16)
+    whole[0] = result
+    swap = pltpu.make_async_remote_copy(
+        src_ref=whole.at[0], dst_ref=theirs.at[0], send_sem=sm.at[0], recv_sem=rm.at[0],
+        device_id={"sp": mate}, device_id_type=MESH)
+    swap.start()
+    first = to_peers("tp", n, lambda peer: whole.at[0], lambda k: whole.at[k], s2, r2)
+    mine, other = side * positions, (1 - side) * positions
+    rows_ref[span(me, rows, mine), :] = result
+    swap.wait()
+    later = to_peers("tp", n, lambda peer: theirs.at[0], lambda k: theirs.at[k], s3, r3)
+    rows_ref[span(me, rows, other), :] = theirs[0]
+    for k in range(1, n):
+        first[k - 1].wait()
+        rows_ref[span(lax.rem(me + n - k, n), rows, mine), :] = whole[k]
+    return later, lambda k: rows_ref.at[span(lax.rem(me + n - k, n), rows, other)]
+
+
+def last_kernel(n, n_sp, part_ref, res_ref, gain_ref, out_ref, got_a, got_b, away, home, s1, r1, s2, r2, sm, rm):
+    me = lax.axis_index("tp")
+    sp = lax.axis_index("sp")
+    m = n_sp // 2
+    side, mate = sp // m, lax.rem(sp + m, n_sp)
+    rows = res_ref.shape[0]
+    positions = rows * n
+    barrier = pltpu.get_barrier_semaphore()
+    for k in range(1, n):
+        pl.semaphore_signal(barrier, inc=1, device_id={"tp": lax.rem(me + k, n)}, device_id_type=MESH)
+    pl.semaphore_signal(barrier, inc=1, device_id={"sp": mate}, device_id_type=MESH)
+    pl.semaphore_wait(barrier, n)
+    mine, other = side * positions, (1 - side) * positions
+    out_first = to_peers("tp", n, lambda p: part_ref.at[span(p, rows, other)], lambda k: got_a.at[k - 1], s1, r1)
+    in_later = to_peers("tp", n, lambda p: part_ref.at[span(p, rows, mine)], lambda k: got_b.at[k - 1], s2, r2)
+    total = part_ref[span(me, rows, other), :].astype(F32)
+    for k in range(1, n):
+        out_first[k - 1].wait()
+        total = total + got_a[k - 1].astype(F32)
+    away[...] = total.astype(BF16)
+    swap = pltpu.make_async_remote_copy(
+        src_ref=away, dst_ref=home, send_sem=sm.at[0], recv_sem=rm.at[0], device_id={"sp": mate}, device_id_type=MESH)
+    swap.start()
+    total = part_ref[span(me, rows, mine), :].astype(F32) + deep_alpha * res_ref[...].astype(F32)
+    for k in range(1, n):
+        in_later[k - 1].wait()
+        total = total + got_b[k - 1].astype(F32)
+    swap.wait()
+    out_ref[...] = normalize(total + home[...].astype(F32), gain_ref[...]).astype(BF16)
+
+
+def last(part, res, gain):
+    n, n_sp = lax.axis_size("tp"), lax.axis_size("sp")
+    rows, width = res.shape
+    dma = pltpu.SemaphoreType.DMA
+    return pl.pallas_call(
+        functools.partial(last_kernel, n, n_sp),
+        out_shape=jax.ShapeDtypeStruct((rows, width), BF16),
+        in_specs=vmem(3),
+        out_specs=pl.BlockSpec(memory_space=pltpu.VMEM),
+        scratch_shapes=[pltpu.VMEM((n - 1, rows, width), BF16), pltpu.VMEM((n - 1, rows, width), BF16),
+                        pltpu.VMEM((rows, width), BF16), pltpu.VMEM((rows, width), BF16),
+                        dma((n - 1,)), dma((n - 1,)), dma((n - 1,)), dma((n - 1,)), dma((1,)), dma((1,))],
+        compiler_params=pltpu.CompilerParams(collective_id=5, has_side_effects=True),
+        name="last_sum",
+    )(part, res, gain.reshape(1, -1))
+
+
+def front_kernel(half, width, n, n_tp, half_of, pair_first, early,
                  u_ref, pace_ref, rows_ref, in_ref, out_ref, feed_ref, wo_ref, res_ref, gain_ref,
                  gate_ref, value_ref, down_ref,
                  whole_ref, gate_all, value_all, down_all,
-                 flow, dec, sf, sb, pf, pb, tot, mine, far, cin, acc, part, got, whole,
-                 s0, r0, s1, r1, s2, r2, gsend, grecv, glocal):
+                 flow, dec, sf, sb, pf, pb, tot, mine, far, cin, acc, part, got, whole, theirs,
+                 s0, r0, s1, r1, s2, r2, s3, r3, sm, rm, gsend, grecv, glocal, csend, crecv):
     me = lax.axis_index("sp")
     tp = lax.axis_index("tp")
     barrier = pltpu.get_barrier_semaphore()
@@ -411,10 +460,11 @@
         pl.semaphore_signal(barrier, inc=1, device_id={"tp": lax.rem(tp + k, n_tp)}, device_id_type=MESH)
     pl.semaphore_wait(barrier, n - 1 + n_tp - 1)
 
-    weights = Gather(n, (gate_ref, value_ref, down_ref), (gate_all, value_all, down_all), parts, pair_first,
-                     gsend, grecv, glocal)
-    total = len(weights.items)
-    weights.begin(0, early)
+    weights = Gather(n, half_of, (gate_ref, value_ref, down_ref), (gate_all, value_all, down_all), pair_first,
+                     gsend, grecv, glocal, csend, crecv)
+    count = len(half_of)
+    for i in range(early):
+        weights.begin(i)
     scan_kernel(half, width, u_ref, pace_ref, rows_ref, in_ref, sf, sb, pf, pb, tot, flow, dec)
     carry_ends(tot, mine)
 
@@ -427,7 +477,10 @@
     def _(k):
         shared(k).start()
 
-    weights.begin(early, total)
+    for i in range(early, count):
+        weights.begin(i)
+    for w in range(count):
+        weights.cross(w, me).start()
     weights.begin_local()
 
     @pl.loop(1, n)
@@ -436,7 +489,19 @@
 
     carry_starts(tot, far, cin, me, n)
     readout_kernel(half, width, sf, sb, pf, pb, cin, out_ref, u_ref, feed_ref, wo_ref, part, acc)
-    settle_body("tp", n_tp, True, part, res_ref, gain_ref, whole_ref, got, whole, s1, r1, s2, r2)
+    for i in pair_first:
+        weights.second(i)
+    weights.pump([i for i in range(count) if i not in pair_first])
+    later, place = mix_rows(n_tp, weights.mate, weights.side, part, res_ref, gain_ref, whole_ref, got, whole, theirs,
+                            s1, r1, s2, r2, s3, r3, sm, rm)
+    for w in range(count):
+        weights.cross(w, weights.mate).wait_recv()
+        weights.begin(count + w)
+    for k in range(1, n_tp):
+        later[k - 1].wait()
+        place(k)[...] = theirs[k]
+    weights.pump(list(pair_first))
+    weights.pump([count + w for w in range(count)])
     weights.finish()
 
 
@@ -459,19 +524,23 @@
     in_cols = jnp.tile(in_cols, (1, 1, reps))
     out_rows = out_map.reshape(2, chans, 2, half).transpose(0, 2, 3, 1).reshape(4, half, chans)
     out_rows = jnp.tile(out_rows, (1, reps, 1))
-    parts = 2 if n <= 16 else 1
-    pair_first = ((2, 0),) if parts == 2 else ()
-    items = 3 * parts
-    slots = 4 * (n // 2 - 1) + 1
+    hidden = w_gate.shape[1]
+    share = -(-hidden // (2 * LANES)) * LANES
+    half_of = ((1, share), (1, share), (0, share))
+    pair_first = (0,)
+    items = 6
+    slots = 4 * (n // 4 - 1) + 1
     dma = pltpu.SemaphoreType.DMA
     own = positions // n_tp
     big = pltpu.VMEM((2, positions, flat), F32)
     anywhere = pl.BlockSpec(memory_space=pl.ANY)
     shards_of = (w_gate, w_value, w_down)
     return pl.pallas_call(
-        functools.partial(front_kernel, half, width, n, n_tp, parts, pair_first, min(2, items)),
-        out_shape=(jax.ShapeDtypeStruct((positions, model), BF16),)
-        + tuple(jax.ShapeDtypeStruct((n,) + w.shape, BF16) for w in shards_of),
+        functools.partial(front_kernel, half, width, n, n_tp, half_of, pair_first, 2),
+        out_shape=(jax.ShapeDtypeStruct((2 * positions, model), BF16),)
+        + tuple(jax.ShapeDtypeStruct(
+            (n,) + tuple(size if d == dim else c for d, c in enumerate(w.shape)), BF16)
+            for w, (dim, size) in zip(shards_of, half_of)),
         in_specs=vmem(9) + [anywhere] * 3,
         out_specs=tuple(vmem(1) + [anywhere] * 3),
         scratch_shapes=[
@@ -481,8 +550,10 @@
             pltpu.VMEM((4, SUB, flat), F32), pltpu.VMEM((positions, chans), F32),
             pltpu.VMEM((positions, model), BF16),
             pltpu.VMEM((n_tp - 1, own, model), BF16), pltpu.VMEM((n_tp, own, model), BF16),
+            pltpu.VMEM((n_tp, own, model), BF16),
             dma((n - 1,)), dma((n - 1,)), dma((n_tp - 1,)), dma((n_tp - 1,)), dma((n_tp - 1,)), dma((n_tp - 1,)),
-            dma((items, slots)), dma((items, slots)), dma((3,)),
+            dma((n_tp - 1,)), dma((n_tp - 1,)), dma((1,)), dma((1,)),
+            dma((items, slots)), dma((items, slots)), dma((3,)), dma((3,)), dma((3,)),
         ],
         compiler_params=pltpu.CompilerParams(collective_id=3, has_side_effects=True),
         cost_estimate=pl.CostEstimate(flops=4 * 10**9, bytes_accessed=10**7, transcendentals=0),
@@ -493,9 +564,15 @@
 
 def edges(gated):
     n = lax.axis_size("sp")
-    before = lax.ppermute(gated[-1:], "sp", [(i, i + 1) for i in range(n - 1)])
-    after = lax.ppermute(gated[:1], "sp", [(i + 1, i) for i in range(n - 1)])
-    return jnp.concatenate([before, gated, after], axis=0)
+    m = n // 2
+    place = lax.rem(lax.axis_index("sp"), m)
+    ring = [(s * m + b, s * m + (b + 1) % m) for s in range(2) for b in range(m)]
+    before = lax.ppermute(gated[:, -1:], "sp", ring)
+    after = lax.ppermute(gated[:, :1], "sp", [(j, i) for i, j in ring])
+    zero = jnp.zeros_like(before[:1])
+    before = jnp.where(place == 0, jnp.concatenate([zero, before[:1]]), before)
+    after = jnp.where(place == m - 1, jnp.concatenate([after[1:], zero]), after)
+    return jnp.concatenate([before, gated, after], axis=1)
 
 
 def shards(residual, ssm_input, in_map, out_map, damping, log_step, frequency, pacing, feedthrough,
@@ -505,17 +582,26 @@
     rows, gate_all, value_all, down_all = front(
         residual, ssm_input, in_map, out_map, damping, log_step, frequency, pacing, feedthrough, w_out,
         gain_mix, w_gate, w_value, w_down)
-    gate_all = gate_all.reshape(-1, w_gate.shape[1])
-    value_all = value_all.reshape(-1, w_value.shape[1])
-    gated = jnp.dot(rows, gate_all, preferred_element_type=F32).astype(BF16)
-    padded = edges(gated).astype(F32)
-    values = jnp.dot(rows, value_all, preferred_element_type=F32).astype(BF16).astype(F32)
-    smoothed = conv_taps[0] * padded[:-2] + conv_taps[1] * padded[1:-1] + conv_taps[2] * padded[2:]
-    hidden = (jax.nn.gelu(smoothed) * values).astype(BF16)
+    model = residual.shape[1]
+    m = lax.axis_size("sp") // 2
+    side = lax.axis_index("sp") // m
+    share = gate_all.shape[2]
+    start = side * (conv_taps.shape[1] - share)
+    overlap = 2 * share - conv_taps.shape[1]
+    taps = lax.dynamic_slice_in_dim(conv_taps, start, share, 1)
+    gated = jnp.dot(rows, gate_all.reshape(model, share), preferred_element_type=F32).astype(BF16)
+    padded = edges(gated.reshape(2, positions, share)).astype(F32)
+    values = jnp.dot(rows, value_all.reshape(model, share), preferred_element_type=F32).astype(BF16)
+    values = values.reshape(2, positions, share).astype(F32)
+    smoothed = taps[0] * padded[:, :-2] + taps[1] * padded[:, 1:-1] + taps[2] * padded[:, 2:]
+    hidden = jax.nn.gelu(smoothed) * values
+    unit = lax.broadcasted_iota(jnp.int32, (1, 1, share), 2)
+    hidden = jnp.where(jnp.logical_and(side == 1, unit < overlap), 0.0, hidden).astype(BF16)
+    hidden = hidden.reshape(2 * positions, share)
     parts = jnp.einsum("th,nhc->tnc", hidden, down_all, preferred_element_type=F32).astype(BF16)
-    parts = parts.reshape(positions, -1)
-    kept = lax.dynamic_slice_in_dim(rows, lax.axis_index("tp") * own_rows, own_rows, 0)
-    return settle(parts, kept, gain_ffn, "tp", False, 5)
+    parts = parts.reshape(2 * positions, model)
+    kept = lax.dynamic_slice_in_dim(rows, side * positions + lax.axis_index("tp") * own_rows, own_rows, 0)
+    return last(parts, kept, gain_ffn)
 
 
 def solution(mesh):

time: 238 us -> 200 us (0.84)
  Pallas kernels: 202 us -> 168 us
  local copies, waits for them, and re-layouts: 12.1 us -> 16.3 us
  starting transfers between devices: 5.68 us -> 2.07 us
  matrix products: 13.4 us -> 10.4 us
  waiting for transfers between devices: 2.48 us -> 0.01 us
    pallas_call x2, Pallas kernels: 202 us -> 168 us  [the longest x1 138 us: front(): pl.pallas_call(functools.partial(front_kernel, half, width, n, n_tp, half...]
    dot_general x1, matrix products: 8.62 us -> 1.84 us  [shards(): jnp.einsum('th,nhc->tnc', hidden, down_all, preferred_element_type=F32)]
    dot_general x1 -> x2, matrix products: 4.77 us -> 8.61 us  [the longest x1 4.31 us: shards(): jnp.dot(rows, gate_all.reshape(model, share), preferred_element_type=F32)]
    ppermute x2, starting transfers between devices: 5.68 us -> 2.07 us  [the longest x1 2.01 us: edges(): before = lax.ppermute(gated[:, -1:], 'sp', ring)]
    ppermute x2, waiting for transfers between devices: 2.48 us -> 0.01 us  [the longest x1 0.01 us: edges(): after = lax.ppermute(gated[:, :1], 'sp', [(j, i) for i, j in ring])]
  transfers between devices with their start and end apart: 2 -> 2, of which waited for: 1 -> 0; matrix products, arithmetic and copies ran while one was open for 1% -> 3% of each run, Pallas kernels for 0% -> 0%
where the time goes in v3:
time: 200 us; the launch traced here: 199 us
  Pallas kernels  168 us (84%)
  local copies, waits for them, and re-layouts  16.3 us (8%)
  matrix products  10.4 us (5%)
  starting transfers between devices  2.07 us (1%)
  other arithmetic  2.05 us (1%)
    pallas_call x1, Pallas kernels, front(): pl.pallas_call(functools.partial(front_kernel, half, width, n, n_tp, half...  138 us
    pallas_call x1, Pallas kernels, last(): pl.pallas_call(functools.partial(last_kernel, n, n_sp), out_shape=jax.Sha...  30.7 us
    dot_general x1, matrix products, shards(): jnp.dot(rows, gate_all.reshape(model, share), preferred_element_type=F32)  4.31 us
    dot_general x1, matrix products, shards(): jnp.dot(rows, value_all.reshape(model, share), preferred_element_type=F32)  4.3 us
  transfers between devices with their start and end apart: 2, of which 0 were waited for; matrix products, arithmetic and copies ran while one was open for 3% of the time, Pallas kernels for 0%

profile of v3, /device:TPU:0, one launch (start us, length us, event | category | flops | bytes accessed | tf_op | source)
XLA Modules:
  0.0 199.3 jit_solution(10623938201397584054)
XLA Ops:
  0.0 1.7 copy.36
  1.7 0.8 reshape.78
  2.6 0.7 exp.3
  3.4 0.8 stack.23
  4.2 0.7 negate_divide_fusion
  5.1 1.0 reshape.79
  6.4 0.8 copy.30.in_ref
  7.2 0.1 reshape.80
  7.5 0.6 stack.26.rows_ref
  8.1 0.7 mul.83.pace_ref
  8.9 0.7 tile.24
  9.6 137.5 %front.1 = (bf16[512,2048]{1,0:T(8,128)(2,1)}, bf16[8,256,768]{2,1,0:T(8,128)(2,1)}, bf16[8,256,768]{2,1,0:T(8,128)(2,1)}, bf16[8,768,256]{2,1,0:T(8,128)(2,1)}) custom-call(bf16[256,256]{1,0:T(8,128)(2,1)} %bitcast.47, f32[256,128]{1,0:T(8,128)} %mul.83.pace_ref, f32[5,1024]{1,0:T(8,128)} %stack.26.rows_ref, bf16[4,256,128]{2,1,0:T(8,128)(2,1)} %copy.30.in_ref, ...), custom_call_target="tpu_custom_call" | custom-call | flops 4000000000 | bytes 10000000 | tf_op jit(solution)/shard_map/front/pallas_call | solution.py:538
  147.1 4.3 %convolution_convert_fusion.2 = bf16[512,768]{1,0:T(8,128)(2,1)S(1)} fusion(bf16[512,2048]{1,0:T(8,128)(2,1)} %get-tuple-element.9, bf16[2048,768]{1,0:T(8,128)(2,1)} %bitcast.53), kind=kOutput, calls=%fused_computation.18 | convolution fusion | flops 1611005952 | bytes 6029312 | tf_op jit(solution)/shard_map/dot_general | solution.py:592
  151.5 2.0 %collective-permute-start = (bf16[2,1,768]{2,1,0:T(2,128)(2,1)S(1)}, bf16[2,1,768]{2,1,0:T(2,128)(2,1)S(1)}, u32[]{:S(2)}, u32[]{:S(2)}) collective-permute-start(bf16[2,1,768]{2,1,0:T(2,128)(2,1)S(1)} %get-tuple-element.16), channel_id=1, source_target_pairs={{0,4},{4,8},{8,12},{12,0},{16,20},{20,24},{24,28},{28,16},{1,5},{5... | collective-permute-start | bytes 9224 | tf_op jit(solution)/shard_map/ppermute | solution.py:570
  153.5 4.3 %convolution_convert_fusion.1 = bf16[512,768]{1,0:T(8,128)(2,1)S(1)} fusion(bf16[512,2048]{1,0:T(8,128)(2,1)} %get-tuple-element.9, bf16[2048,768]{1,0:T(8,128)(2,1)} %bitcast.52), kind=kOutput, calls=%fused_computation.17 | convolution fusion | flops 1611005952 | bytes 6029312 | tf_op jit(solution)/shard_map/dot_general | solution.py:594
  157.8 1.7 constant_dynamic-slice_fusion.res_ref
  159.5 0.9 dynamic-slice_reduce_fusion.2
  160.5 0.2 maximum_convert_fusion
  160.7 1.1 fusion.9
  161.8 0.8 copy-done.1
  162.6 1.8 convolution_convert_fusion
  164.4 2.5 %copy.34.part_ref = bf16[512,2048]{1,0:T(8,128)(2,1)} copy(bf16[512,2048]{0,1:T(8,128)(2,1)S(1)} %bitcast.35) | data formatting | bytes 4194304 | tf_op jit(solution)/shard_map/reshape | solution.py:602
  166.9 30.7 %last_sum.1 = bf16[64,2048]{1,0:T(8,128)(2,1)} custom-call(bf16[512,2048]{1,0:T(8,128)(2,1)} %copy.34.part_ref, bf16[64,2048]{1,0:T(8,128)(2,1)} %constant_dynamic-slice_fusion.res_ref, f32[1,2048]{1,0:T(1,128)} %bitcast.49), custom_call_target="tpu_custom_call" | custom-call | tf_op jit(solution)/shard_map/last_sum/pallas_call | solution.py:432
  197.7 1.7 copy.38
  (22 shorter events, 1.0 us)
Async XLA Ops:
  0.0 7.2 %copy-start = (bf16[2,16,16,128]{3,2,1,0:T(8,128)(2,1)S(1)}, bf16[2,16,16,128]{3,2,1,0:T(8,128)(2,1)}, u32[]{:S(2)}) copy-start(bf16[2,16,16,128]{3,2,1,0:T(8,128)(2,1)} %param.19) | copy-start | bytes 393220
  151.4 9.0 %collective-permute-start.1 = (bf16[2,1,768]{2,1,0:T(2,128)(2,1)S(1)}, bf16[2,1,768]{2,1,0:T(2,128)(2,1)S(1)}, u32[]{:S(2)}, u32[]{:S(2)}) collective-permute-start(bf16[2,1,768]{2,1,0:T(2,128)(2,1)S(1)} %get-tuple-element.17), channel_id=1, source_target_pairs={{4,0},{8,4},{12,8},{0,12},{20,16},{24,20},{28,24},{16,28},{5,1},{9... | collective-permute-start | bytes 9224 | tf_op jit(solution)/shard_map/ppermute | solution.py:571
  151.5 9.0 %collective-permute-start = (bf16[2,1,768]{2,1,0:T(2,128)(2,1)S(1)}, bf16[2,1,768]{2,1,0:T(2,128)(2,1)S(1)}, u32[]{:S(2)}, u32[]{:S(2)}) collective-permute-start(bf16[2,1,768]{2,1,0:T(2,128)(2,1)S(1)} %get-tuple-element.16), channel_id=1, source_target_pairs={{0,4},{4,8},{8,12},{12,0},{16,20},{20,24},{24,28},{28,16},{1,5},{5... | collective-permute-start | bytes 9224 | tf_op jit(solution)/shard_map/ppermute | solution.py:570
  160.7 1.9 copy-start.1

commit v4 on v3

--- a/solution.py
+++ b/solution.py
@@ -367,7 +367,8 @@
     return pl.ds(pl.multiple_of(base + who * rows, rows), rows)
 
 
-def mix_rows(n, mate, side, part, res_ref, gain_ref, rows_ref, got, whole, theirs, s1, r1, s2, r2, s3, r3, sm, rm):
+def mix_rows(n, mate, side, part, res_ref, gain_ref, rows_ref, got, whole, theirs, s1, r1, s2, r2, s3, r3, sm, rm,
+             pass_on):
     me = lax.axis_index("tp")
     positions = part.shape[0]
     rows = positions // n
@@ -385,6 +386,7 @@
     first = to_peers("tp", n, lambda peer: whole.at[0], lambda k: whole.at[k], s2, r2)
     mine, other = side * positions, (1 - side) * positions
     rows_ref[span(me, rows, mine), :] = result
+    pass_on()
     swap.wait()
     later = to_peers("tp", n, lambda peer: theirs.at[0], lambda k: theirs.at[k], s3, r3)
     rows_ref[span(me, rows, other), :] = theirs[0]
@@ -394,33 +396,60 @@
     return later, lambda k: rows_ref.at[span(lax.rem(me + n - k, n), rows, other)]
 
 
-def last_kernel(n, n_sp, part_ref, res_ref, gain_ref, out_ref, got_a, got_b, away, home, s1, r1, s2, r2, sm, rm):
+def last_kernel(n, n_sp, part_ref, res_ref, gain_ref, out_ref, pair_got, stage, got, away, home,
+                s1, r1, s2, r2, sm, rm):
     me = lax.axis_index("tp")
     sp = lax.axis_index("sp")
     m = n_sp // 2
     side, mate = sp // m, lax.rem(sp + m, n_sp)
+    outer, parity = me // 2, lax.rem(me, 2)
+    pairs = n // 2
+    partner = outer * 2 + 1 - parity
     rows = res_ref.shape[0]
     positions = rows * n
     barrier = pltpu.get_barrier_semaphore()
-    for k in range(1, n):
-        pl.semaphore_signal(barrier, inc=1, device_id={"tp": lax.rem(me + k, n)}, device_id_type=MESH)
+
+    def at(k):
+        return lax.rem(outer + k, pairs) * 2
+
+    pl.semaphore_signal(barrier, inc=1, device_id={"tp": partner}, device_id_type=MESH)
+    for k in range(1, pairs):
+        pl.semaphore_signal(barrier, inc=1, device_id={"tp": at(k) + parity}, device_id_type=MESH)
     pl.semaphore_signal(barrier, inc=1, device_id={"sp": mate}, device_id_type=MESH)
-    pl.semaphore_wait(barrier, n)
-    mine, other = side * positions, (1 - side) * positions
-    out_first = to_peers("tp", n, lambda p: part_ref.at[span(p, rows, other)], lambda k: got_a.at[k - 1], s1, r1)
-    in_later = to_peers("tp", n, lambda p: part_ref.at[span(p, rows, mine)], lambda k: got_b.at[k - 1], s2, r2)
-    total = part_ref[span(me, rows, other), :].astype(F32)
-    for k in range(1, n):
-        out_first[k - 1].wait()
-        total = total + got_a[k - 1].astype(F32)
+    pl.semaphore_wait(barrier, 1 + pairs)
+    bases = ((1 - side) * positions, side * positions)
+    near, far, kept = {}, {}, []
+    order = list(range(1, pairs)) + [0]
+    for b, base in enumerate(bases):
+        for k in order:
+            near[b, k] = pltpu.make_async_remote_copy(
+                src_ref=part_ref.at[span(at(k) + 1 - parity, rows, base)], dst_ref=pair_got.at[b, k],
+                send_sem=s1.at[b, k], recv_sem=r1.at[b, k], device_id={"tp": partner}, device_id_type=MESH)
+            near[b, k].start()
+    for b, base in enumerate(bases):
+        for k in order:
+            near[b, k].wait()
+            both = part_ref[span(at(k) + parity, rows, base), :].astype(F32) + pair_got[b, k].astype(F32)
+            if k == 0:
+                kept.append(both)
+                continue
+            stage[b, k] = both.astype(BF16)
+            far[b, k] = pltpu.make_async_remote_copy(
+                src_ref=stage.at[b, k], dst_ref=got.at[b, k], send_sem=s2.at[b, k], recv_sem=r2.at[b, k],
+                device_id={"tp": at(k) + parity}, device_id_type=MESH)
+            far[b, k].start()
+    total = kept[0]
+    for k in range(1, pairs):
+        far[0, k].wait()
+        total = total + got[0, k].astype(F32)
     away[...] = total.astype(BF16)
     swap = pltpu.make_async_remote_copy(
         src_ref=away, dst_ref=home, send_sem=sm.at[0], recv_sem=rm.at[0], device_id={"sp": mate}, device_id_type=MESH)
     swap.start()
-    total = part_ref[span(me, rows, mine), :].astype(F32) + deep_alpha * res_ref[...].astype(F32)
-    for k in range(1, n):
-        in_later[k - 1].wait()
-        total = total + got_b[k - 1].astype(F32)
+    total = kept[1] + deep_alpha * res_ref[...].astype(F32)
+    for k in range(1, pairs):
+        far[1, k].wait()
+        total = total + got[1, k].astype(F32)
     swap.wait()
     out_ref[...] = normalize(total + home[...].astype(F32), gain_ref[...]).astype(BF16)
 
@@ -428,15 +457,16 @@
 def last(part, res, gain):
     n, n_sp = lax.axis_size("tp"), lax.axis_size("sp")
     rows, width = res.shape
-    dma = pltpu.SemaphoreType.DMA
+    dma = pltpu.SemaphoreType.DMA((2, n // 2))
+    one = pltpu.SemaphoreType.DMA((1,))
+    quads = pltpu.VMEM((2, n // 2, rows, width), BF16)
+    row = pltpu.VMEM((rows, width), BF16)
     return pl.pallas_call(
         functools.partial(last_kernel, n, n_sp),
         out_shape=jax.ShapeDtypeStruct((rows, width), BF16),
         in_specs=vmem(3),
         out_specs=pl.BlockSpec(memory_space=pltpu.VMEM),
-        scratch_shapes=[pltpu.VMEM((n - 1, rows, width), BF16), pltpu.VMEM((n - 1, rows, width), BF16),
-                        pltpu.VMEM((rows, width), BF16), pltpu.VMEM((rows, width), BF16),
-                        dma((n - 1,)), dma((n - 1,)), dma((n - 1,)), dma((n - 1,)), dma((1,)), dma((1,))],
+        scratch_shapes=[quads, quads, quads, row, row, dma, dma, dma, dma, one, one],
         compiler_params=pltpu.CompilerParams(collective_id=5, has_side_effects=True),
         name="last_sum",
     )(part, res, gain.reshape(1, -1))
@@ -477,10 +507,11 @@
     def _(k):
         shared(k).start()
 
+    for w in range(early):
+        weights.cross(w, me).start()
     for i in range(early, count):
         weights.begin(i)
-    for w in range(count):
-        weights.cross(w, me).start()
+        weights.cross(i, me).start()
     weights.begin_local()
 
     @pl.loop(1, n)
@@ -492,11 +523,14 @@
     for i in pair_first:
         weights.second(i)
     weights.pump([i for i in range(count) if i not in pair_first])
+
+    def pass_on():
+        for w in range(count):
+            weights.cross(w, weights.mate).wait_recv()
+            weights.begin(count + w)
+
     later, place = mix_rows(n_tp, weights.mate, weights.side, part, res_ref, gain_ref, whole_ref, got, whole, theirs,
-                            s1, r1, s2, r2, s3, r3, sm, rm)
-    for w in range(count):
-        weights.cross(w, weights.mate).wait_recv()
-        weights.begin(count + w)
+                            s1, r1, s2, r2, s3, r3, sm, rm, pass_on)
     for k in range(1, n_tp):
         later[k - 1].wait()
         place(k)[...] = theirs[k]

time: 200 us -> 182 us (0.910)
  Pallas kernels: 168 us -> 150 us
    pallas_call x1, Pallas kernels: 138 us -> 124 us  [front(): pl.pallas_call(functools.partial(front_kernel, half, width, n, n_tp, half...]
    pallas_call x1, Pallas kernels: 30.7 us -> 26.8 us  [last(): pl.pallas_call(functools.partial(last_kernel, n, n_sp), out_shape=jax.Sha...]
  transfers between devices with their start and end apart: 2 -> 2, of which waited for: 0 -> 0; matrix products, arithmetic and copies ran while one was open for 3% -> 4% of each run, Pallas kernels for 0% -> 0%
where the time goes in v4:
time: 182 us; the launch traced here: 181 us
  Pallas kernels  150 us (82%)
  local copies, waits for them, and re-layouts  16.3 us (9%)
  matrix products  10.4 us (6%)
  starting transfers between devices  2.07 us (1%)
  other arithmetic  2.05 us (1%)
    pallas_call x1, Pallas kernels, front(): pl.pallas_call(functools.partial(front_kernel, half, width, n, n_tp, half...  124 us
    pallas_call x1, Pallas kernels, last(): pl.pallas_call(functools.partial(last_kernel, n, n_sp), out_shape=jax.Sha...  26.8 us
    dot_general x1, matrix products, shards(): jnp.dot(rows, gate_all.reshape(model, share), preferred_element_type=F32)  4.31 us
    dot_general x1, matrix products, shards(): jnp.dot(rows, value_all.reshape(model, share), preferred_element_type=F32)  4.3 us
  transfers between devices with their start and end apart: 2, of which 0 were waited for; matrix products, arithmetic and copies ran while one was open for 4% of the time, Pallas kernels for 0%

profile of v4, /device:TPU:0, one launch (start us, length us, event | category | flops | bytes accessed | tf_op | source)
XLA Modules:
  0.0 181.5 jit_solution(11527332282773452009)
XLA Ops:
  0.0 1.7 copy.36
  1.7 0.8 reshape.78
  2.6 0.7 exp.3
  3.4 0.8 stack.23
  4.2 0.7 negate_divide_fusion
  5.1 1.0 reshape.79
  6.4 0.8 copy.30.in_ref
  7.2 0.1 reshape.80
  7.5 0.6 stack.26.rows_ref
  8.1 0.7 mul.83.pace_ref
  8.9 0.7 tile.24
  9.6 123.6 %front.1 = (bf16[512,2048]{1,0:T(8,128)(2,1)}, bf16[8,256,768]{2,1,0:T(8,128)(2,1)}, bf16[8,256,768]{2,1,0:T(8,128)(2,1)}, bf16[8,768,256]{2,1,0:T(8,128)(2,1)}) custom-call(bf16[256,256]{1,0:T(8,128)(2,1)} %bitcast.47, f32[256,128]{1,0:T(8,128)} %mul.83.pace_ref, f32[5,1024]{1,0:T(8,128)} %stack.26.rows_ref, bf16[4,256,128]{2,1,0:T(8,128)(2,1)} %copy.30.in_ref, ...), custom_call_target="tpu_custom_call" | custom-call | flops 4000000000 | bytes 10000000 | tf_op jit(solution)/shard_map/front/pallas_call | solution.py:572
  133.1 4.3 %convolution_convert_fusion.2 = bf16[512,768]{1,0:T(8,128)(2,1)S(1)} fusion(bf16[512,2048]{1,0:T(8,128)(2,1)} %get-tuple-element.9, bf16[2048,768]{1,0:T(8,128)(2,1)} %bitcast.53), kind=kOutput, calls=%fused_computation.18 | convolution fusion | flops 1611005952 | bytes 6029312 | tf_op jit(solution)/shard_map/dot_general | solution.py:626
  137.5 2.0 %collective-permute-start = (bf16[2,1,768]{2,1,0:T(2,128)(2,1)S(1)}, bf16[2,1,768]{2,1,0:T(2,128)(2,1)S(1)}, u32[]{:S(2)}, u32[]{:S(2)}) collective-permute-start(bf16[2,1,768]{2,1,0:T(2,128)(2,1)S(1)} %get-tuple-element.16), channel_id=1, source_target_pairs={{0,4},{4,8},{8,12},{12,0},{16,20},{20,24},{24,28},{28,16},{1,5},{5... | collective-permute-start | bytes 9224 | tf_op jit(solution)/shard_map/ppermute | solution.py:604
  139.5 4.3 %convolution_convert_fusion.1 = bf16[512,768]{1,0:T(8,128)(2,1)S(1)} fusion(bf16[512,2048]{1,0:T(8,128)(2,1)} %get-tuple-element.9, bf16[2048,768]{1,0:T(8,128)(2,1)} %bitcast.52), kind=kOutput, calls=%fused_computation.17 | convolution fusion | flops 1611005952 | bytes 6029312 | tf_op jit(solution)/shard_map/dot_general | solution.py:628
  143.9 1.7 constant_dynamic-slice_fusion.res_ref
  145.6 0.9 dynamic-slice_reduce_fusion.2
  146.6 0.2 maximum_convert_fusion
  146.8 1.1 fusion.9
  147.9 0.8 copy-done.1
  148.6 1.8 %convolution_convert_fusion = bf16[512,8,256]{0,2,1:T(8,128)(2,1)S(1)} fusion(bf16[512,768,1]{1,0,2:T(8,128)(2,1)S(1)} %bitcast.42, bf16[8,768,256]{2,1,0:T(8,128)(2,1)S(1)} %copy-done.1), kind=kOutput, calls=%fused_computation.1 | convolution fusion | flops 1611661312 | bytes 6029312 | tf_op jit(solution)/shard_map/th,nhc->tnc/dot_general | solution.py:635
  150.5 2.5 %copy.34.part_ref = bf16[512,2048]{1,0:T(8,128)(2,1)} copy(bf16[512,2048]{0,1:T(8,128)(2,1)S(1)} %bitcast.35) | data formatting | bytes 4194304 | tf_op jit(solution)/shard_map/reshape | solution.py:636
  153.0 26.8 %last_sum.1 = bf16[64,2048]{1,0:T(8,128)(2,1)} custom-call(bf16[512,2048]{1,0:T(8,128)(2,1)} %copy.34.part_ref, bf16[64,2048]{1,0:T(8,128)(2,1)} %constant_dynamic-slice_fusion.res_ref, f32[1,2048]{1,0:T(1,128)} %bitcast.49), custom_call_target="tpu_custom_call" | custom-call | tf_op jit(solution)/shard_map/last_sum/pallas_call | solution.py:464
  179.8 1.7 copy.38
  (22 shorter events, 1.0 us)
Async XLA Ops:
  0.0 7.2 %copy-start = (bf16[2,16,16,128]{3,2,1,0:T(8,128)(2,1)S(1)}, bf16[2,16,16,128]{3,2,1,0:T(8,128)(2,1)}, u32[]{:S(2)}) copy-start(bf16[2,16,16,128]{3,2,1,0:T(8,128)(2,1)} %param.19) | copy-start | bytes 393220
  137.5 9.0 %collective-permute-start.1 = (bf16[2,1,768]{2,1,0:T(2,128)(2,1)S(1)}, bf16[2,1,768]{2,1,0:T(2,128)(2,1)S(1)}, u32[]{:S(2)}, u32[]{:S(2)}) collective-permute-start(bf16[2,1,768]{2,1,0:T(2,128)(2,1)S(1)} %get-tuple-element.17), channel_id=1, source_target_pairs={{4,0},{8,4},{12,8},{0,12},{20,16},{24,20},{28,24},{16,28},{5,1},{9... | collective-permute-start | bytes 9224 | tf_op jit(solution)/shard_map/ppermute | solution.py:605
  137.5 9.0 %collective-permute-start = (bf16[2,1,768]{2,1,0:T(2,128)(2,1)S(1)}, bf16[2,1,768]{2,1,0:T(2,128)(2,1)S(1)}, u32[]{:S(2)}, u32[]{:S(2)}) collective-permute-start(bf16[2,1,768]{2,1,0:T(2,128)(2,1)S(1)} %get-tuple-element.16), channel_id=1, source_target_pairs={{0,4},{4,8},{8,12},{12,0},{16,20},{20,24},{24,28},{28,16},{1,5},{5... | collective-permute-start | bytes 9224 | tf_op jit(solution)/shard_map/ppermute | solution.py:604
  146.8 1.9 %copy-start.1 = (bf16[8,768,256]{2,1,0:T(8,128)(2,1)S(1)}, bf16[8,768,256]{2,1,0:T(8,128)(2,1)}, u32[]{:S(2)}) copy-start(bf16[8,768,256]{2,1,0:T(8,128)(2,1)} %get-tuple-element.12) | copy-start | bytes 9437188
